TPU v7x, 32 devices: a whole 2x2x4 slice. The times are simulated.
32 devices in a mesh: ep: 8 (over z, x), tp: 4 (over y, core).
Axes of the slice: x: 2, y: 2, z: 4, core: 2. Of those that a mesh axis runs over, the one named last changes fastest.
Arguments:
- tokens: bfloat16 [1024, 4096], P('ep', 'tp'), may hold values from -16 to 16
- expert_ids: int32 [1024, 2], P('ep'), may hold values from 0 to 7, as said below
- group_weight: float32 [1024], P('ep'), may hold values from 0.25 to 1
- expert_weight: float32 [1024, 2], P('ep'), may hold values from 0.1 to 1
- w_gate: bfloat16 [8, 4096, 512], P('ep', None, 'tp'), may hold values from -0.09375 to 0.09375
- w_up: bfloat16 [8, 4096, 512], P('ep', None, 'tp'), may hold values from -0.09375 to 0.09375
- w_down: bfloat16 [8, 512, 4096], P('ep', None, 'tp'), may hold values from -0.5 to 0.5
- norm_gain: float32 [4096], P('tp'), may hold values from 0.1 to 1.9
- norm_bias: float32 [4096], P('tp'), may hold values from -3 to 3
Outputs:
- normed: bfloat16 [1024, 4096], P('ep', 'tp')
Inputs may be any that keep to these rules, and one draw needn't show every extreme that they name: `expert_ids`: each row names 2 different experts of one group, a group being 2 consecutive ids; in the rows of one ep index each group is named by a 4-th of the rows. In the rows of one ep index no expert is named more than 32 times, and in every group one expert is named exactly 32 times in the rows of every ep index.
All inputs are finite; a program needn't handle non-finite values.
Results may differ from a plain program's by a relative error of at most 0.0045.
Values may be sent and summed in bfloat16 or wider, within the bound.
A program may use at most 64 MiB of HBM per device.

v0:
```python
import functools

import jax
import jax.numpy as jnp
from jax import lax
from jax.experimental import pallas as pl
from jax.experimental.pallas import tpu as pltpu
from jax.sharding import PartitionSpec as P

D = 4096
GROUPS = 4
TOP_K = 2


residual_scale = 2.0**0.5
norm_eps = 1e-05


def on_device(
    tokens, expert_ids, group_weight, expert_weight, w_gate, w_up, w_down, norm_gain, norm_bias
):
    tok_count = tokens.shape[0]
    expert_count = lax.axis_size("ep")
    capacity = min(tok_count // GROUPS, 3 * TOP_K * tok_count // (2 * expert_count))
    pair_count = tok_count * TOP_K
    flat_ids = expert_ids.reshape(pair_count)
    one_hot = (flat_ids[:, None] == jnp.arange(expert_count, dtype=jnp.int32)[None, :]).astype(
        jnp.float32
    )
    earlier = (jnp.arange(pair_count)[:, None] > jnp.arange(pair_count)[None, :]).astype(
        jnp.float32
    )
    prior_counts = jnp.dot(
        earlier, one_hot, preferred_element_type=jnp.float32, precision=lax.Precision.HIGHEST
    )
    slot_index = jnp.sum(prior_counts * one_hot, axis=1).astype(jnp.int32)
    position = flat_ids * capacity + slot_index
    owner_token = jnp.arange(pair_count, dtype=jnp.int32) // TOP_K
    slot_table = (
        jnp.full((expert_count * capacity,), tok_count, jnp.int32).at[position].set(owner_token)
    )
    gate_local = w_gate[0]
    up_local = w_up[0]
    down_local = w_down[0]
    padded = jnp.concatenate([tokens, jnp.zeros((1, tokens.shape[1]), tokens.dtype)], axis=0)
    outgoing = padded[slot_table].reshape(expert_count, capacity, tokens.shape[1])
    arrived = lax.all_to_all(outgoing, "ep", split_axis=0, concat_axis=0, tiled=True)
    sources, slot_count, slice_width = arrived.shape
    row_block = arrived.reshape(sources * slot_count, slice_width)
    row_piece = lax.all_gather(row_block, "tp", axis=1, tiled=True)
    gate_sum = jnp.dot(row_piece, gate_local, preferred_element_type=jnp.float32)
    up_sum = jnp.dot(row_piece, up_local, preferred_element_type=jnp.float32)
    hidden = (jax.nn.silu(gate_sum) * up_sum).astype(jnp.bfloat16)
    result = jnp.dot(
        lax.all_gather(hidden, "tp", axis=1, tiled=True),
        down_local,
        preferred_element_type=jnp.float32,
    )
    result = result.astype(jnp.bfloat16).reshape(sources, slot_count, down_local.shape[1])
    returned = lax.all_to_all(result, "ep", split_axis=0, concat_axis=0, tiled=True)
    flat_rows = returned.reshape(expert_count * capacity, returned.shape[2])
    picked = flat_rows[position].reshape(tok_count, TOP_K, returned.shape[2]).astype(jnp.float32)
    share_weight = (
        group_weight[:, None] * expert_weight / jnp.sum(expert_weight, axis=1, keepdims=True)
    )
    routed = jnp.einsum("tk,tkd->td", share_weight, picked)
    mixed = residual_scale * tokens.astype(jnp.float32) + routed
    first_sum, second_sum = lax.psum((jnp.sum(mixed, axis=1), jnp.sum(mixed * mixed, axis=1)), "tp")
    center = first_sum / D
    spread = second_sum / D - center * center
    centered = mixed - center[:, None]
    normed = (
        centered * lax.rsqrt(spread + norm_eps)[:, None] * norm_gain[None, :] + norm_bias[None, :]
    )
    return normed.astype(jnp.bfloat16)


MESH = pl.DeviceIdType.MESH
F32 = jnp.float32
BF16 = jnp.bfloat16
(TO_PLANE, SHARES, CORE_OWN, ACROSS_X, ACROSS_Y, CORE_X, CORE_Y, RELAY_X, RELAY_Y,
 CORE_RX, CORE_RY, HIDDEN_0, HIDDEN_1, RESULT, BACK, STATS, ACROSS_X2, ACROSS_Y2, RESULT_2,
 BACK_2, TO_PLANE_2) = range(21)
KINDS = 21


def flip(value, bits):
    bit = 1
    while bit <= bits:
        if bits & bit:
            value = value + bit - 2 * bit * lax.rem(lax.div(value, bit), 2)
        bit *= 2
    return value


def layer_kernel(
    n_plane, n_tp,
    tokens_hbm, ids_hbm, group_hbm, expert_hbm, gate_hbm, up_hbm, down_hbm,
    mixed_out, columns_out,
    tokens_ref, ids_ref, group_ref, expert_ref, mixed_ref,
    w_in, w_out, outgoing, share_out, share_in, rows, hidden, own_part, result_out, result_in,
    back_out, back_in, stats, send_sem, recv_sem, load_sem,
):
    ep = lax.axis_index("ep")
    q = lax.axis_index("tp")
    z, x = lax.div(ep, 2), lax.rem(ep, 2)
    ox = 1 - x
    q_core, q_y, q_diag = flip(q, 1), flip(q, 2), flip(q, 3)
    core_peer, y_peer, diag_peer = (ep, q_core), (ep, q_y), (ep, q_diag)
    x_peer = (z * 2 + ox, q)

    def plane_peer(d):
        return (flip(z, d) * 2 + x, q)

    tok, width = tokens_ref.shape
    cap = tok // n_plane
    half = cap // 2
    inner = gate_hbm.shape[2]

    inputs = [
        pltpu.make_async_copy(source, target, load_sem.at[3 + i])
        for i, (source, target) in enumerate((
            (ids_hbm, ids_ref), (tokens_hbm, tokens_ref), (group_hbm, group_ref),
            (expert_hbm, expert_ref),
        ))
    ]
    for load in inputs:
        load.start()

    barrier = pltpu.get_barrier_semaphore()
    partners = [plane_peer(d) for d in range(1, n_plane)] + [x_peer, core_peer, y_peer, diag_peer]
    for peer in partners:
        pl.semaphore_signal(barrier, inc=1, device_id=peer, device_id_type=MESH)

    loads = [
        pltpu.make_async_copy(gate_hbm.at[0], w_in.at[:, pl.ds(0, inner)], load_sem.at[0]),
        pltpu.make_async_copy(up_hbm.at[0], w_in.at[:, pl.ds(inner, inner)], load_sem.at[1]),
        pltpu.make_async_copy(down_hbm.at[0], w_out, load_sem.at[2]),
    ]
    for load in loads:
        load.start()

    inputs[0].wait()
    first = ids_ref[0:1, :]
    group_row = (first >> 1).astype(F32)
    on_lanes = jnp.broadcast_to(group_row, (tok, tok))
    on_rows = jnp.transpose(on_lanes)
    ii = lax.broadcasted_iota(jnp.int32, (tok, tok), 0)
    jj = lax.broadcasted_iota(jnp.int32, (tok, tok), 1)
    same = on_lanes == on_rows
    zero, one = jnp.zeros((tok, tok), F32), jnp.ones((tok, tok), F32)
    rank_row = jnp.sum(jnp.where(same & (ii < jj), one, zero), axis=0, keepdims=True)
    rank_col = jnp.sum(jnp.where(same & (jj < ii), one, zero), axis=1, keepdims=True)
    place_row = group_row * cap + rank_row
    place_col = on_rows[:, 0:1] * cap + rank_col
    to_slot = jnp.broadcast_to(place_row, (tok, tok)) == ii.astype(F32)
    to_token = jnp.broadcast_to(place_col, (tok, tok)) == jj.astype(F32)

    inputs[1].wait()
    sorted_rows = jnp.dot(
        jnp.where(to_slot, one, zero).astype(BF16), tokens_ref[...], preferred_element_type=F32
    ).astype(BF16)
    outgoing[...] = sorted_rows.reshape(n_plane, cap, width)
    rows[q, x, z] = outgoing[z]

    inputs[2].wait()
    inputs[3].wait()
    weights = expert_ref[...]
    share = group_ref[...] * weights / jnp.sum(weights, axis=0, keepdims=True)
    even = (first & 1) == 0
    share_a = jnp.where(even, share[0:1, :], share[1:2, :])
    share_b = jnp.where(even, share[1:2, :], share[0:1, :])
    slot_a = jnp.sum(jnp.where(to_slot, jnp.broadcast_to(share_a, (tok, tok)), zero), axis=1, keepdims=True)
    slot_b = jnp.sum(jnp.where(to_slot, jnp.broadcast_to(share_b, (tok, tok)), zero), axis=1, keepdims=True)
    lane = lax.broadcasted_iota(jnp.int32, (tok, 128), 1)
    share_out[...] = jnp.where(lane < 64, slot_a, slot_b).reshape(n_plane, cap, 128)
    share_in[z] = share_out[z]

    pl.semaphore_wait(barrier, len(partners))

    started = []

    def copy(src, dst, kind, j, peer):
        return pltpu.make_async_remote_copy(
            src_ref=src, dst_ref=dst, send_sem=send_sem.at[kind, j], recv_sem=recv_sem.at[kind, j],
            device_id=peer, device_id_type=MESH,
        )

    def send(src, dst, kind, j, peer):
        c = copy(src, dst, kind, j, peer)
        c.start()
        started.append(c)

    def arrived(dst, kind, j):
        copy(dst, dst, kind, j, core_peer).wait_recv()

    low, high = pl.ds(0, half), pl.ds(half, half)
    for d in range(1, n_plane):
        for part, kind in ((low, TO_PLANE), (high, TO_PLANE_2)):
            send(outgoing.at[flip(z, d), part], rows.at[q, x, z, part], kind, d, plane_peer(d))

    def spread_own(j):
        block = rows.at[q, x, flip(z, j)]
        if j:
            arrived(block.at[low], TO_PLANE, j)
        send(block.at[low], block.at[low], ACROSS_X, j, x_peer)
        if j:
            send(block.at[low], block.at[low], ACROSS_Y2, j, y_peer)
            arrived(block.at[high], TO_PLANE_2, j)
        send(block.at[high], block.at[high], ACROSS_Y, j, y_peer)
        send(block.at[high], block.at[high], ACROSS_X2, j, x_peer)
        if not j:
            send(block.at[low], block.at[low], ACROSS_Y2, j, y_peer)
        send(block, block, CORE_OWN, j, core_peer)

    def pass_on(j):
        zz = flip(z, j)
        over_x, over_y = rows.at[q, ox, zz], rows.at[q_y, x, zz]
        arrived(over_x.at[low], ACROSS_X, j)
        send(over_x.at[low], over_x.at[low], RELAY_Y, j, y_peer)
        arrived(over_y.at[high], ACROSS_Y, j)
        send(over_y.at[high], over_y.at[high], RELAY_X, j, x_peer)
        arrived(over_x.at[high], ACROSS_X2, j)
        send(over_x, over_x, CORE_X, j, core_peer)
        arrived(over_y.at[low], ACROSS_Y2, j)
        send(over_y, over_y, CORE_Y, j, core_peer)

    def pass_relayed(j):
        block = rows.at[q_y, ox, flip(z, j)]
        arrived(block.at[low], RELAY_Y, j)
        send(block.at[low], block.at[low], CORE_RY, j, core_peer)
        arrived(block.at[high], RELAY_X, j)
        send(block.at[high], block.at[high], CORE_RX, j, core_peer)

    for step in range(n_plane + 1):
        if step < n_plane:
            spread_own(step)
        if step >= 1:
            pass_on(step - 1)
        if step >= 2:
            pass_relayed(step - 2)

    for d in range(1, n_plane):
        send(share_out.at[flip(z, d)], share_in.at[z], SHARES, d, plane_peer(d))

    def sums_of(column, quarter):
        part = rows[quarter, column].reshape(tok, width)
        w = w_in[pl.ds(pl.multiple_of(quarter * width, width), width), :]
        return jnp.dot(part, w, preferred_element_type=F32)

    def finish_hidden(total, column, kind):
        gate, up = total[:, :inner], total[:, inner:]
        hidden[column, q] = (gate / (1.0 + jnp.exp(-gate)) * up).astype(BF16)
        block = hidden.at[column, q]
        for d, peer in ((2, y_peer), (3, diag_peer), (1, core_peer)):
            send(block, block, kind, d, peer)

    def project(column, kind):
        for d in range(1, n_tp):
            arrived(hidden.at[column, flip(q, d)], kind, d)
        h = jnp.concatenate([hidden[column, t] for t in range(n_tp)], axis=1)
        return jnp.dot(h, w_out[...], preferred_element_type=F32).astype(BF16)

    loads[0].wait()
    loads[1].wait()
    total = sums_of(x, q) + sums_of(x, q_y)
    other = sums_of(ox, q)
    for j in range(n_plane):
        arrived(rows.at[q_core, x, flip(z, j)], CORE_OWN, j)
        arrived(rows.at[q_diag, x, flip(z, j)], CORE_Y, j)
    total = total + sums_of(x, q_core) + sums_of(x, q_diag)
    finish_hidden(total, x, HIDDEN_0)
    pass_relayed(n_plane - 1)
    for j in range(n_plane):
        arrived(rows.at[q_core, ox, flip(z, j)], CORE_X, j)
    other = other + sums_of(ox, q_core) + sums_of(ox, q_y)
    for j in range(n_plane):
        block = rows.at[q_diag, ox, flip(z, j)]
        arrived(block.at[low], CORE_RY, j)
        arrived(block.at[high], CORE_RX, j)
    other = other + sums_of(ox, q_diag)
    finish_hidden(other, ox, HIDDEN_1)

    loads[2].wait()
    for d in range(1, n_plane):
        arrived(share_in.at[flip(z, d)], SHARES, d)
    shares = share_in[...].reshape(tok, 128)
    is_first = x == 0
    share_own = jnp.where(is_first, shares[:, 0:1], shares[:, 64:65])
    share_other = jnp.where(is_first, shares[:, 64:65], shares[:, 0:1])
    own_part[...] = (project(x, HIDDEN_0).astype(F32) * share_own).reshape(n_plane, cap, width)
    share_in[...] = jnp.broadcast_to(share_other, (tok, 128)).reshape(n_plane, cap, 128)

    result_out[...] = project(ox, HIDDEN_1).reshape(n_plane, cap, width)
    order = tuple(range(n_plane - 1, -1, -1))
    pieces = ((low, 0, RESULT, BACK), (high, half, RESULT_2, BACK_2))
    for j in order:
        zz = flip(z, j)
        for part, _, there, _ in pieces:
            send(result_out.at[zz, part], result_in.at[zz, part], there, j, x_peer)
    for j in order:
        zz = flip(z, j)
        for part, at, there, home in pieces:
            arrived(result_in.at[zz, part], there, j)
            scaled = result_in[zz, at:at + half].astype(F32) * share_in[zz, at:at + half][:, 0:1]
            mixed_rows = (own_part[zz, at:at + half] + scaled).astype(BF16)
            if j:
                back_out[zz, at:at + half] = mixed_rows
                send(back_out.at[zz, part], back_in.at[z, part], home, j, plane_peer(j))
            else:
                back_in[z, at:at + half] = mixed_rows
    for j in order:
        if j:
            for part, _, _, home in pieces:
                arrived(back_in.at[flip(z, j), part], home, j)
    routed = jnp.dot(
        jnp.where(to_token, one, zero).astype(BF16),
        back_in[...].reshape(tok, width),
        preferred_element_type=F32,
    )
    mixed = residual_scale * tokens_ref[...].astype(F32) + routed
    mixed_ref[...] = mixed
    keep = pltpu.make_async_copy(mixed_ref, mixed_out, load_sem.at[7])
    keep.start()
    total_col = jnp.sum(mixed, axis=1, keepdims=True)
    centered = mixed - total_col / width
    square_col = jnp.sum(centered * centered, axis=1, keepdims=True)
    lane = lax.broadcasted_iota(jnp.int32, (tok, 128), 1)
    stats[q] = jnp.transpose(jnp.where(lane == 0, total_col, square_col))[0:8, :]
    for d, peer in ((3, diag_peer), (2, y_peer), (1, core_peer)):
        send(stats.at[q], stats.at[q], STATS, d, peer)
    for d in range(1, n_tp):
        arrived(stats.at[flip(q, d)], STATS, d)
    pieces = [stats[t] for t in range(n_tp)]
    full = width * n_tp
    center = sum(p[0:1, :] for p in pieces) / full
    spread = sum(p[1:2, :] + width * jnp.square(p[0:1, :] / width - center) for p in pieces) / full
    scale = lax.rsqrt(spread + norm_eps)
    sub = lax.broadcasted_iota(jnp.int32, (128, tok), 0)
    columns_out[...] = jnp.transpose(jnp.where(sub == 0, center, scale))
    keep.wait()
    for c in started:
        c.wait_send()


def norm_kernel(mixed_ref, columns_ref, gain_ref, bias_ref, out_ref):
    center, scale = columns_ref[:, 0:1], columns_ref[:, 1:2]
    out_ref[...] = (
        (mixed_ref[...] - center) * scale * gain_ref[...] + bias_ref[...]
    ).astype(BF16)


def pair_groups(
    tokens, expert_ids, group_weight, expert_weight, w_gate, w_up, w_down, norm_gain, norm_bias
):
    tok, width = tokens.shape
    n_plane = lax.axis_size("ep") // TOP_K
    n_tp = lax.axis_size("tp")
    cap = tok // n_plane
    inner = w_gate.shape[2]
    vmem = pl.BlockSpec(memory_space=pltpu.VMEM)
    hbm = pl.BlockSpec(memory_space=pltpu.HBM)
    mixed, columns = pl.pallas_call(
        functools.partial(layer_kernel, n_plane, n_tp),
        out_shape=(
            jax.ShapeDtypeStruct((tok, width), F32), jax.ShapeDtypeStruct((tok, 128), F32)
        ),
        in_specs=[hbm] * 7,
        out_specs=(pl.BlockSpec(memory_space=pl.ANY), vmem),
        scratch_shapes=[
            pltpu.VMEM((tok, width), BF16),
            pltpu.VMEM((TOP_K, tok), jnp.int32),
            pltpu.VMEM((1, tok), F32),
            pltpu.VMEM((TOP_K, tok), F32),
            pltpu.VMEM((tok, width), F32),
            pltpu.VMEM((w_gate.shape[1], 2 * inner), BF16),
            pltpu.VMEM(w_down.shape[1:], BF16),
            pltpu.VMEM((n_plane, cap, width), BF16),
            pltpu.VMEM((n_plane, cap, 128), F32),
            pltpu.VMEM((n_plane, cap, 128), F32),
            pltpu.VMEM((n_tp, 2, n_plane, cap, width), BF16),
            pltpu.VMEM((2, n_tp, tok, inner), BF16),
            pltpu.VMEM((n_plane, cap, width), F32),
            pltpu.VMEM((n_plane, cap, width), BF16),
            pltpu.VMEM((n_plane, cap, width), BF16),
            pltpu.VMEM((n_plane, cap, width), BF16),
            pltpu.VMEM((n_plane, cap, width), BF16),
            pltpu.VMEM((n_tp, 8, tok), F32),
            pltpu.SemaphoreType.DMA((KINDS, 4)),
            pltpu.SemaphoreType.DMA((KINDS, 4)),
            pltpu.SemaphoreType.DMA((8,)),
        ],
        compiler_params=pltpu.CompilerParams(
            collective_id=0, has_side_effects=True, vmem_limit_bytes=53 * 2**20
        ),
        name="layer",
    )(
        *(
            pltpu.with_memory_space_constraint(a, pltpu.HBM)
            for a in (
                tokens, expert_ids.T, group_weight[None, :], expert_weight.T, w_gate, w_up, w_down
            )
        )
    )
    return pl.pallas_call(
        norm_kernel,
        out_shape=jax.ShapeDtypeStruct((tok, width), BF16),
        in_specs=[vmem] * 4,
        out_specs=vmem,
        compiler_params=pltpu.CompilerParams(vmem_limit_bytes=8 * 2**20),
        name="norm",
    )(mixed, columns, norm_gain[None, :], norm_bias[None, :])


def solution(mesh):
    n_ep, n_tp = mesh.shape["ep"], mesh.shape["tp"]
    pairs = TOP_K == 2 and n_ep == GROUPS * TOP_K and n_tp == 4
    return jax.shard_map(
        pair_groups if pairs else on_device,
        mesh=mesh,
        in_specs=(
            P("ep", "tp"),
            P("ep", None),
            P("ep"),
            P("ep", None),
            P("ep", None, "tp"),
            P("ep", None, "tp"),
            P("ep", None, "tp"),
            P("tp"),
            P("tp"),
        ),
        out_specs=P("ep", "tp"),
        check_vma=False,
    )
```

profile of v0, /device:TPU:0, one launch (start us, length us, event | category | flops | bytes accessed | tf_op | source)
XLA Modules:
  0.0 41.1 jit_solution(4371462433319868708)
XLA Ops:
  0.0 0.0 copy-start
  0.0 0.0 copy-start.1
  0.0 40.2 %layer.1 = (f32[128,1024]{1,0:T(8,128)S(1)}, f32[128,128]{1,0:T(8,128)S(1)}) custom-call(bf16[128,1024]{1,0:T(8,128)(2,1)} %tokens_hbm.1, s32[2,128]{1,0:T(2,128)} %bitcast.7, f32[1,128]{1,0:T(1,128)} %bitcast.9, f32[2,128]{1,0:T(2,128)} %bitcast.8, bf16[1,4096,128]{2,1,0:T(8,128)(2,1)} %gate_hbm.1, bf16[1,4096,128]{2,1,0:T(8,128)(2,1)} %up_hbm.1, ...), custom_call_target="tpu_custom_call" | custom-call | tf_op jit(solution)/shard_map/layer/pallas_call | solution.py:363
  40.2 0.0 copy-done
  40.2 0.0 copy-done.1
  40.2 0.9 %norm.1 = bf16[128,1024]{1,0:T(8,128)(2,1)} custom-call(f32[128,1024]{1,0:T(8,128)S(1)} %get-tuple-element.7.mixed_ref, f32[128,128]{1,0:T(8,128)S(1)} %get-tuple-element.8.columns_ref, f32[1,1024]{1,0:T(1,128)S(1)} %bitcast.5, f32[1,1024]{1,0:T(1,128)S(1)} %bitcast.6), custom_call_target="tpu_custom_call" | custom-call | tf_op jit(solution)/shard_map/norm/pallas_call | solution.py:405
Async XLA Ops:
  0.0 40.2 %copy-start = (f32[1024]{0:T(1024)S(1)}, f32[1024]{0:T(1024)}, u32[]{:S(2)}) copy-start(f32[1024]{0:T(1024)} %param.16) | copy-start | bytes 12292
  0.0 40.2 %copy-start.1 = (f32[1024]{0:T(1024)S(1)}, f32[1024]{0:T(1024)}, u32[]{:S(2)}) copy-start(f32[1024]{0:T(1024)} %param.17) | copy-start | bytes 12292
where the time goes:
time: 41.2 us; the launch traced here: 41.1 us
  Pallas kernels  41.1 us (100%)
    pallas_call x1, Pallas kernels, pair_groups(): pl.pallas_call(functools.partial(layer_kernel, n_plane, n_tp), out_shape=...  40.2 us
    pallas_call x1, Pallas kernels, pair_groups(): pl.pallas_call(norm_kernel, out_shape=jax.ShapeDtypeStruct((tok, width),...  0.87 us

commit v1 on v0

v1 whole, which is shorter than its diff:
```python
import functools

import jax
import jax.numpy as jnp
from jax import lax
from jax.experimental import pallas as pl
from jax.experimental.pallas import tpu as pltpu
from jax.sharding import PartitionSpec as P

D = 4096
GROUPS = 4
TOP_K = 2


residual_scale = 2.0**0.5
norm_eps = 1e-05


def on_device(
    tokens, expert_ids, group_weight, expert_weight, w_gate, w_up, w_down, norm_gain, norm_bias
):
    tok_count = tokens.shape[0]
    expert_count = lax.axis_size("ep")
    capacity = min(tok_count // GROUPS, 3 * TOP_K * tok_count // (2 * expert_count))
    pair_count = tok_count * TOP_K
    flat_ids = expert_ids.reshape(pair_count)
    one_hot = (flat_ids[:, None] == jnp.arange(expert_count, dtype=jnp.int32)[None, :]).astype(
        jnp.float32
    )
    earlier = (jnp.arange(pair_count)[:, None] > jnp.arange(pair_count)[None, :]).astype(
        jnp.float32
    )
    prior_counts = jnp.dot(
        earlier, one_hot, preferred_element_type=jnp.float32, precision=lax.Precision.HIGHEST
    )
    slot_index = jnp.sum(prior_counts * one_hot, axis=1).astype(jnp.int32)
    position = flat_ids * capacity + slot_index
    owner_token = jnp.arange(pair_count, dtype=jnp.int32) // TOP_K
    slot_table = (
        jnp.full((expert_count * capacity,), tok_count, jnp.int32).at[position].set(owner_token)
    )
    gate_local = w_gate[0]
    up_local = w_up[0]
    down_local = w_down[0]
    padded = jnp.concatenate([tokens, jnp.zeros((1, tokens.shape[1]), tokens.dtype)], axis=0)
    outgoing = padded[slot_table].reshape(expert_count, capacity, tokens.shape[1])
    arrived = lax.all_to_all(outgoing, "ep", split_axis=0, concat_axis=0, tiled=True)
    sources, slot_count, slice_width = arrived.shape
    row_block = arrived.reshape(sources * slot_count, slice_width)
    row_piece = lax.all_gather(row_block, "tp", axis=1, tiled=True)
    gate_sum = jnp.dot(row_piece, gate_local, preferred_element_type=jnp.float32)
    up_sum = jnp.dot(row_piece, up_local, preferred_element_type=jnp.float32)
    hidden = (jax.nn.silu(gate_sum) * up_sum).astype(jnp.bfloat16)
    result = jnp.dot(
        lax.all_gather(hidden, "tp", axis=1, tiled=True),
        down_local,
        preferred_element_type=jnp.float32,
    )
    result = result.astype(jnp.bfloat16).reshape(sources, slot_count, down_local.shape[1])
    returned = lax.all_to_all(result, "ep", split_axis=0, concat_axis=0, tiled=True)
    flat_rows = returned.reshape(expert_count * capacity, returned.shape[2])
    picked = flat_rows[position].reshape(tok_count, TOP_K, returned.shape[2]).astype(jnp.float32)
    share_weight = (
        group_weight[:, None] * expert_weight / jnp.sum(expert_weight, axis=1, keepdims=True)
    )
    routed = jnp.einsum("tk,tkd->td", share_weight, picked)
    mixed = residual_scale * tokens.astype(jnp.float32) + routed
    first_sum, second_sum = lax.psum((jnp.sum(mixed, axis=1), jnp.sum(mixed * mixed, axis=1)), "tp")
    center = first_sum / D
    spread = second_sum / D - center * center
    centered = mixed - center[:, None]
    normed = (
        centered * lax.rsqrt(spread + norm_eps)[:, None] * norm_gain[None, :] + norm_bias[None, :]
    )
    return normed.astype(jnp.bfloat16)


MESH = pl.DeviceIdType.MESH
F32 = jnp.float32
BF16 = jnp.bfloat16
(TO_PLANE, TO_PLANE_2, SHARES, CORE_OWN, ACROSS_X, ACROSS_Y, CORE_X, CORE_Y, RELAY_X, RELAY_Y,
 CORE_RX, CORE_RY, HIDDEN, RESULT, RESULT_2, BACK, BACK_2, ACROSS_X2, ACROSS_Y2) = range(19)
KINDS = 19


def flip(value, bits):
    bit = 1
    while bit <= bits:
        if bits & bit:
            value = value + bit - 2 * bit * lax.rem(lax.div(value, bit), 2)
        bit *= 2
    return value


def layer_kernel(
    n_plane, n_tp,
    tokens_hbm, ids_hbm, group_hbm, expert_hbm, gate_hbm, up_hbm, down_hbm, gain_hbm, bias_hbm,
    normed_out,
    tokens_ref, ids_ref, group_ref, expert_ref, gain_ref, bias_ref,
    w_in, w_out, outgoing, share_out, share_in, share_far, rows, hidden, own_part, result_out,
    result_in, back_out, back_in, stats_out, stats_in,
    send_sem, recv_sem, hidden_send, hidden_recv, stats_send, stats_recv, load_sem, entered,
):
    ep = lax.axis_index("ep")
    q = lax.axis_index("tp")
    z, x = lax.div(ep, 2), lax.rem(ep, 2)
    ox = 1 - x
    q_core, q_y, q_diag = flip(q, 1), flip(q, 2), flip(q, 3)
    core_peer, y_peer, diag_peer = (ep, q_core), (ep, q_y), (ep, q_diag)
    x_peer = (z * 2 + ox, q)

    def at_plane(zz):
        return (zz * 2 + x, q)

    last = n_plane - 1
    inside = lax.div(z * (last - z), 2)
    z1 = 1 + lax.rem(z, 2)
    z3 = last * (1 - lax.div(z, 2))
    z2 = 6 - z - z1 - z3
    outer = last * (z - 1) * inside

    tok, width = tokens_ref.shape
    cap = tok // n_plane
    half = cap // 2
    inner = gate_hbm.shape[2]

    inputs = [
        pltpu.make_async_copy(source, target, load_sem.at[3 + i])
        for i, (source, target) in enumerate((
            (ids_hbm, ids_ref), (tokens_hbm, tokens_ref), (group_hbm, group_ref),
            (expert_hbm, expert_ref), (gain_hbm, gain_ref), (bias_hbm, bias_ref),
        ))
    ]
    for load in inputs:
        load.start()

    barrier = pltpu.get_barrier_semaphore()
    for peer in (at_plane(z1), x_peer, core_peer, y_peer, diag_peer):
        pl.semaphore_signal(barrier, inc=1, device_id=peer, device_id_type=MESH)

    @pl.when(inside == 1)
    def _():
        pl.semaphore_signal(barrier, inc=1, device_id=at_plane(outer), device_id_type=MESH)

    loads = [
        pltpu.make_async_copy(gate_hbm.at[0], w_in.at[:, pl.ds(0, inner)], load_sem.at[0]),
        pltpu.make_async_copy(up_hbm.at[0], w_in.at[:, pl.ds(inner, inner)], load_sem.at[1]),
        pltpu.make_async_copy(down_hbm.at[0], w_out, load_sem.at[2]),
    ]
    for load in loads:
        load.start()

    inputs[0].wait()
    first = ids_ref[0:1, :]
    group_row = (first >> 1).astype(F32)
    on_lanes = jnp.broadcast_to(group_row, (tok, tok))
    on_rows = jnp.transpose(on_lanes)
    ii = lax.broadcasted_iota(jnp.int32, (tok, tok), 0)
    jj = lax.broadcasted_iota(jnp.int32, (tok, tok), 1)
    same = on_lanes == on_rows
    zero, one = jnp.zeros((tok, tok), F32), jnp.ones((tok, tok), F32)
    rank_row = jnp.sum(jnp.where(same & (ii < jj), one, zero), axis=0, keepdims=True)
    rank_col = jnp.sum(jnp.where(same & (jj < ii), one, zero), axis=1, keepdims=True)
    place_row = group_row * cap + rank_row
    place_col = on_rows[:, 0:1] * cap + rank_col
    to_slot = jnp.broadcast_to(place_row, (tok, tok)) == ii.astype(F32)
    to_token = jnp.broadcast_to(place_col, (tok, tok)) == jj.astype(F32)

    inputs[1].wait()
    sorted_rows = jnp.dot(
        jnp.where(to_slot, one, zero).astype(BF16), tokens_ref[...], preferred_element_type=F32
    ).astype(BF16)
    outgoing[...] = sorted_rows.reshape(n_plane, cap, width)
    rows[q, x, z] = outgoing[z]

    inputs[2].wait()
    inputs[3].wait()
    weights = expert_ref[...]
    share = group_ref[...] * weights / jnp.sum(weights, axis=0, keepdims=True)
    even = (first & 1) == 0
    for k in range(2):
        chosen = jnp.where(even, share[k:k + 1, :], share[1 - k:2 - k, :])
        by_token = jnp.transpose(jnp.broadcast_to(chosen, (tok, tok)))
        share_out[k:k + 1, :] = jnp.sum(jnp.where(to_token, by_token, zero), axis=0, keepdims=True)
    share_in[z] = share_out[...]

    pl.semaphore_wait(barrier, 5 + inside)

    def tell(which, peer):
        pl.semaphore_signal(entered.at[which], inc=1, device_id=peer, device_id_type=MESH)

    @pl.when(inside == 1)
    def _():
        tell(0, at_plane(z1))
        tell(0, at_plane(outer))

    started = []

    def copy(src, dst, sems, recvs, peer):
        return pltpu.make_async_remote_copy(
            src_ref=src, dst_ref=dst, send_sem=sems, recv_sem=recvs,
            device_id=peer, device_id_type=MESH,
        )

    def send_between(src, dst, kind, there, here, peer):
        c = copy(src, dst, send_sem.at[kind, there], recv_sem.at[kind, here], peer)
        c.start()
        started.append(c)

    def send(block, kind, zz, peer):
        send_between(block, block, kind, zz, zz, peer)

    def arrived(dst, kind, zz):
        copy(dst, dst, send_sem.at[kind, zz], recv_sem.at[kind, zz], core_peer).wait_recv()

    low, high = pl.ds(0, half), pl.ds(half, half)

    def to_plane(zz):
        for part, kind in ((low, TO_PLANE), (high, TO_PLANE_2)):
            send_between(outgoing.at[zz, part], rows.at[q, x, z, part], kind, zz, z, at_plane(zz))

    def spread_low(zz):
        block = rows.at[q, x, zz]
        arrived(block.at[low], TO_PLANE, zz)
        send(block.at[low], ACROSS_X, zz, x_peer)
        send(block.at[low], ACROSS_Y2, zz, y_peer)

    def spread_high(zz):
        block = rows.at[q, x, zz]
        arrived(block.at[high], TO_PLANE_2, zz)
        send(block.at[high], ACROSS_Y, zz, y_peer)
        send(block.at[high], ACROSS_X2, zz, x_peer)
        send(block, CORE_OWN, zz, core_peer)

    def spread_own():
        block = rows.at[q, x, z]
        send(block.at[low], ACROSS_X, z, x_peer)
        send(block.at[high], ACROSS_Y, z, y_peer)
        send(block.at[high], ACROSS_X2, z, x_peer)
        send(block.at[low], ACROSS_Y2, z, y_peer)
        send(block, CORE_OWN, z, core_peer)

    def pass_on(zz):
        over_x, over_y = rows.at[q, ox, zz], rows.at[q_y, x, zz]
        arrived(over_x.at[low], ACROSS_X, zz)
        send(over_x.at[low], RELAY_Y, zz, y_peer)
        arrived(over_y.at[high], ACROSS_Y, zz)
        send(over_y.at[high], RELAY_X, zz, x_peer)
        arrived(over_x.at[high], ACROSS_X2, zz)
        send(over_x, CORE_X, zz, core_peer)
        arrived(over_y.at[low], ACROSS_Y2, zz)
        send(over_y, CORE_Y, zz, core_peer)

    def pass_relayed(zz):
        block = rows.at[q_y, ox, zz]
        arrived(block.at[low], RELAY_Y, zz)
        send(block.at[low], CORE_RY, zz, core_peer)
        arrived(block.at[high], RELAY_X, zz)
        send(block.at[high], CORE_RX, zz, core_peer)

    def sums_of(zz, quarter):
        part = jnp.concatenate([rows[quarter, x, zz], rows[quarter, ox, zz]], axis=0)
        w = w_in[pl.ds(pl.multiple_of(quarter * width, width), width), :]
        return jnp.dot(part, w, preferred_element_type=F32)

    def make_hidden(zz):
        total = sums_of(zz, q) + sums_of(zz, q_y)
        arrived(rows.at[q_core, x, zz], CORE_OWN, zz)
        arrived(rows.at[q_core, ox, zz], CORE_X, zz)
        total = total + sums_of(zz, q_core)
        arrived(rows.at[q_diag, x, zz], CORE_Y, zz)
        block = rows.at[q_diag, ox, zz]
        arrived(block.at[low], CORE_RY, zz)
        arrived(block.at[high], CORE_RX, zz)
        total = total + sums_of(zz, q_diag)
        gate, up = total[:, :inner], total[:, inner:]
        hidden[zz, q] = (gate / (1.0 + jnp.exp(-gate)) * up).astype(BF16)
        block = hidden.at[zz, q]
        for d, peer in ((2, y_peer), (3, diag_peer), (1, core_peer)):
            c = copy(block, block, hidden_send.at[d, zz], hidden_recv.at[d, zz], peer)
            c.start()
            started.append(c)

    lane = lax.broadcasted_iota(jnp.int32, (cap, 128), 1)
    place = lax.broadcasted_iota(jnp.int32, (cap, 128), 0) + z * cap
    here = lane == place
    none = jnp.zeros((cap, 128), F32)

    def column_of(row):
        return jnp.sum(jnp.where(here, jnp.broadcast_to(row, (cap, 128)), none), axis=1, keepdims=True)

    is_first = x == 0

    def project(zz):
        even_share, odd_share = column_of(share_in[zz, 0:1]), column_of(share_in[zz, 1:2])
        share_own = jnp.where(is_first, even_share, odd_share)
        share_far[zz] = jnp.broadcast_to(jnp.where(is_first, odd_share, even_share), (cap, 128))
        for d in range(1, n_tp):
            block = hidden.at[zz, flip(q, d)]
            copy(block, block, hidden_send.at[d, zz], hidden_recv.at[d, zz], core_peer).wait_recv()
        h = jnp.concatenate([hidden[zz, t] for t in range(n_tp)], axis=1)
        result = jnp.dot(h, w_out[...], preferred_element_type=F32).astype(BF16)
        result_out[zz] = result[cap:]
        for part, kind in ((low, RESULT), (high, RESULT_2)):
            send_between(result_out.at[zz, part], result_in.at[zz, part], kind, zz, zz, x_peer)
        own_part[zz] = result[:cap].astype(F32) * share_own

    def give_back(zz, own=False):
        for part, at, kind, home in ((low, 0, RESULT, BACK), (high, half, RESULT_2, BACK_2)):
            arrived(result_in.at[zz, part], kind, zz)
            scaled = result_in[zz, at:at + half].astype(F32) * share_far[zz, at:at + half][:, 0:1]
            routed = (own_part[zz, at:at + half] + scaled).astype(BF16)
            if own:
                back_in[z, at:at + half] = routed
            else:
                back_out[zz, at:at + half] = routed
                send_between(
                    back_out.at[zz, part], back_in.at[z, part], home, zz, z, at_plane(zz)
                )
        routed = back_in[z] if own else back_out[zz]
        mixed = residual_scale * rows[q, x, zz].astype(F32) + routed.astype(F32)
        total = jnp.sum(mixed, axis=1, keepdims=True)
        centered = mixed - total / width
        square = jnp.sum(centered * centered, axis=1, keepdims=True)
        for k, column in enumerate((total, square)):
            stats_out[zz, k:k + 1] = jnp.sum(
                jnp.where(here, jnp.broadcast_to(column, (cap, 128)), none), axis=0, keepdims=True
            )
        for d in (2, 3, 1, 0):
            if own and not d:
                stats_in[z, q] = stats_out[z]
                continue
            c = copy(
                stats_out.at[zz], stats_in.at[z, q], stats_send.at[d, zz], stats_recv.at[d, z],
                (zz * 2 + x, flip(q, d)),
            )
            c.start()
            started.append(c)

    to_plane(z1)
    spread_own()
    pl.semaphore_wait(entered.at[0], 1)

    @pl.when(inside == 1)
    def _():
        tell(1, at_plane(outer))

    to_plane(z2)

    @pl.when(inside == 0)
    def _():
        pl.semaphore_wait(entered.at[1], 1)

    to_plane(z3)
    for zz in (z1, z2, z3):
        send_between(share_out, share_in.at[z], SHARES, zz, z, at_plane(zz))

    spread_low(z1)
    pass_on(z)
    spread_high(z1)
    spread_low(z2)
    spread_high(z2)
    loads[0].wait()
    loads[1].wait()
    pass_relayed(z)
    pass_on(z1)
    make_hidden(z)
    pass_relayed(z1)
    pass_on(z2)
    spread_low(z3)
    spread_high(z3)
    make_hidden(z1)
    loads[2].wait()
    for zz in (z1, z2, z3):
        arrived(share_in.at[zz], SHARES, zz)
    pass_relayed(z2)
    project(z)
    pass_on(z3)
    make_hidden(z2)
    project(z1)
    pass_relayed(z3)
    give_back(z, own=True)
    make_hidden(z3)
    project(z2)
    give_back(z1)
    project(z3)
    give_back(z2)
    give_back(z3)

    for zz in (z1, z2, z3):
        arrived(back_in.at[zz, low], BACK, zz)
        arrived(back_in.at[zz, high], BACK_2, zz)
    routed = jnp.dot(
        jnp.where(to_token, one, zero).astype(BF16),
        back_in[...].reshape(tok, width),
        preferred_element_type=F32,
    )
    mixed = residual_scale * tokens_ref[...].astype(F32) + routed
    for d in range(n_tp):
        for zz in (z, z1, z2, z3) if d else (z1, z2, z3):
            block = stats_in.at[zz, flip(q, d)]
            copy(block, block, stats_send.at[d, zz], stats_recv.at[d, zz], core_peer).wait_recv()
    pieces = [sum(stats_in[zz, t] for zz in range(n_plane)) for t in range(n_tp)]
    full = width * n_tp
    center = sum(p[0:1] for p in pieces) / full
    spread = sum(p[1:2] + width * jnp.square(p[0:1] / width - center) for p in pieces) / full
    scale = lax.rsqrt(spread + norm_eps)
    center, scale = (
        jnp.sum(jnp.where(to_token, jnp.broadcast_to(row, (tok, tok)), zero), axis=1, keepdims=True)
        for row in (center, scale)
    )
    inputs[4].wait()
    inputs[5].wait()
    normed_out[...] = (
        (mixed - center) * scale * gain_ref[...] + bias_ref[...]
    ).astype(BF16)
    for c in started:
        c.wait_send()


def pair_groups(
    tokens, expert_ids, group_weight, expert_weight, w_gate, w_up, w_down, norm_gain, norm_bias
):
    tok, width = tokens.shape
    n_plane = lax.axis_size("ep") // TOP_K
    n_tp = lax.axis_size("tp")
    cap = tok // n_plane
    inner = w_gate.shape[2]
    vmem = pl.BlockSpec(memory_space=pltpu.VMEM)
    hbm = pl.BlockSpec(memory_space=pltpu.HBM)
    return pl.pallas_call(
        functools.partial(layer_kernel, n_plane, n_tp),
        out_shape=jax.ShapeDtypeStruct((tok, width), BF16),
        in_specs=[hbm] * 9,
        out_specs=vmem,
        scratch_shapes=[
            pltpu.VMEM((tok, width), BF16),
            pltpu.VMEM((TOP_K, tok), jnp.int32),
            pltpu.VMEM((1, tok), F32),
            pltpu.VMEM((TOP_K, tok), F32),
            pltpu.VMEM((1, width), F32),
            pltpu.VMEM((1, width), F32),
            pltpu.VMEM((w_gate.shape[1], 2 * inner), BF16),
            pltpu.VMEM(w_down.shape[1:], BF16),
            pltpu.VMEM((n_plane, cap, width), BF16),
            pltpu.VMEM((2, tok), F32),
            pltpu.VMEM((n_plane, 2, tok), F32),
            pltpu.VMEM((n_plane, cap, 128), F32),
            pltpu.VMEM((n_tp, 2, n_plane, cap, width), BF16),
            pltpu.VMEM((n_plane, n_tp, 2 * cap, inner), BF16),
            pltpu.VMEM((n_plane, cap, width), F32),
            pltpu.VMEM((n_plane, cap, width), BF16),
            pltpu.VMEM((n_plane, cap, width), BF16),
            pltpu.VMEM((n_plane, cap, width), BF16),
            pltpu.VMEM((n_plane, cap, width), BF16),
            pltpu.VMEM((n_plane, 2, tok), F32),
            pltpu.VMEM((n_plane, n_tp, 2, tok), F32),
            pltpu.SemaphoreType.DMA((KINDS, n_plane)),
            pltpu.SemaphoreType.DMA((KINDS, n_plane)),
            pltpu.SemaphoreType.DMA((n_tp, n_plane)),
            pltpu.SemaphoreType.DMA((n_tp, n_plane)),
            pltpu.SemaphoreType.DMA((n_tp, n_plane)),
            pltpu.SemaphoreType.DMA((n_tp, n_plane)),
            pltpu.SemaphoreType.DMA((9,)),
            pltpu.SemaphoreType.REGULAR((2,)),
        ],
        compiler_params=pltpu.CompilerParams(
            collective_id=0, has_side_effects=True, vmem_limit_bytes=53 * 2**20
        ),
        name="layer",
    )(
        *(
            pltpu.with_memory_space_constraint(a, pltpu.HBM)
            for a in (
                tokens, expert_ids.T, group_weight[None, :], expert_weight.T, w_gate, w_up, w_down,
                norm_gain[None, :], norm_bias[None, :],
            )
        )
    )


def solution(mesh):
    n_ep, n_tp = mesh.shape["ep"], mesh.shape["tp"]
    pairs = TOP_K == 2 and n_ep == GROUPS * TOP_K and n_tp == 4
    return jax.shard_map(
        pair_groups if pairs else on_device,
        mesh=mesh,
        in_specs=(
            P("ep", "tp"),
            P("ep", None),
            P("ep"),
            P("ep", None),
            P("ep", None, "tp"),
            P("ep", None, "tp"),
            P("ep", None, "tp"),
            P("tp"),
            P("tp"),
        ),
        out_specs=P("ep", "tp"),
        check_vma=False,
    )
```

time: 41.2 us -> 39 us (0.947)
  Pallas kernels: 41.1 us -> 38.1 us
  local copies, waits for them, and re-layouts: 0.01 us -> 0.71 us
    pallas_call x1, Pallas kernels: 40.2 us -> 38.1 us  [pair_groups(): pl.pallas_call(functools.partial(layer_kernel, n_plane, n_tp), out_shape=...]
    pallas_call x1 -> x0, Pallas kernels: 0.87 us -> none  [pair_groups(): pl.pallas_call(norm_kernel, out_shape=jax.ShapeDtypeStruct((tok, width),...]
    unnamed x4 -> x1, local copies, waits for them, and re-layouts: 0.01 us -> 0.71 us
where the time goes in v1:
time: 39 us; the launch traced here: 38.9 us
  Pallas kernels  38.1 us (98%)
  local copies, waits for them, and re-layouts  0.71 us (2%)
    pallas_call x1, Pallas kernels, pair_groups(): pl.pallas_call(functools.partial(layer_kernel, n_plane, n_tp), out_shape=...  38.1 us

profile of v1, /device:TPU:0, one launch (start us, length us, event | category | flops | bytes accessed | tf_op | source)
XLA Modules:
  0.0 38.9 jit_solution(17381278328420222034)
XLA Ops:
  0.0 38.1 %layer.1 = bf16[128,1024]{1,0:T(8,128)(2,1)S(1)} custom-call(bf16[128,1024]{1,0:T(8,128)(2,1)} %tokens_hbm.1, s32[2,128]{1,0:T(2,128)} %bitcast.7, f32[1,128]{1,0:T(1,128)} %bitcast.9, f32[2,128]{1,0:T(2,128)} %bitcast.8, bf16[1,4096,128]{2,1,0:T(8,128)(2,1)} %gate_hbm.1, bf16[1,4096,128]{2,1,0:T(8,128)(2,1)} %up_hbm.1, bf16[1,512,1024]{2,1,0:T(8,128)(2,1)} %down_hbm.1, ...), custom_call_target="tpu_custom_call" | custom-call | tf_op jit(solution)/shard_map/layer/pallas_call | solution.py:431
  38.1 0.7 %copy.11 = bf16[128,1024]{1,0:T(8,128)(2,1)} copy(bf16[128,1024]{1,0:T(8,128)(2,1)S(1)} %layer.1) | data formatting | bytes 524288

commit v2 on v1

--- a/solution.py
+++ b/solution.py
@@ -78,9 +78,11 @@
 MESH = pl.DeviceIdType.MESH
 F32 = jnp.float32
 BF16 = jnp.bfloat16
-(TO_PLANE, TO_PLANE_2, SHARES, CORE_OWN, ACROSS_X, ACROSS_Y, CORE_X, CORE_Y, RELAY_X, RELAY_Y,
- CORE_RX, CORE_RY, HIDDEN, RESULT, RESULT_2, BACK, BACK_2, ACROSS_X2, ACROSS_Y2) = range(19)
-KINDS = 19
+(TO_PLANE, TO_PLANE_2, ACROSS_X, ACROSS_Y, ACROSS_X2, ACROSS_Y2, RELAY_X, RELAY_Y, CORE, HIDDEN,
+ RESULT, RESULT_2) = range(12)
+KINDS = 12
+BACK, SHARES, STATS = range(3)
+TO_CORE, IN_PLANE, OFF_PLANE, RESULTS, HIDDENS, SHARE, STAT = range(7)
 
 
 def flip(value, bits):
@@ -99,7 +101,7 @@
     tokens_ref, ids_ref, group_ref, expert_ref, gain_ref, bias_ref,
     w_in, w_out, outgoing, share_out, share_in, share_far, rows, hidden, own_part, result_out,
     result_in, back_out, back_in, stats_out, stats_in,
-    send_sem, recv_sem, hidden_send, hidden_recv, stats_send, stats_recv, load_sem, entered,
+    send_sem, recv_sem, once_sem, load_sem, entered,
 ):
     ep = lax.axis_index("ep")
     q = lax.axis_index("tp")
@@ -113,11 +115,13 @@
         return (zz * 2 + x, q)
 
     last = n_plane - 1
-    inside = lax.div(z * (last - z), 2)
-    z1 = 1 + lax.rem(z, 2)
-    z3 = last * (1 - lax.div(z, 2))
-    z2 = 6 - z - z1 - z3
-    outer = last * (z - 1) * inside
+    bottom = lax.div(last - z, last)
+    t1 = bottom
+    t2 = n_plane // 2 - lax.div(z, 2)
+    t3 = last - lax.div(z, last)
+    z1 = z - 1 + 2 * bottom
+    z3 = last - last * lax.div(z, last)
+    z2 = n_plane * last // 2 - z - z1 - z3
 
     tok, width = tokens_ref.shape
     cap = tok // n_plane
@@ -135,12 +139,16 @@
         load.start()
 
     barrier = pltpu.get_barrier_semaphore()
-    for peer in (at_plane(z1), x_peer, core_peer, y_peer, diag_peer):
+    for peer in (x_peer, core_peer, y_peer, diag_peer):
         pl.semaphore_signal(barrier, inc=1, device_id=peer, device_id_type=MESH)
-
-    @pl.when(inside == 1)
-    def _():
-        pl.semaphore_signal(barrier, inc=1, device_id=at_plane(outer), device_id_type=MESH)
+    for zz in range(n_plane):
+
+        @pl.when((zz > z) | (zz == z - 1))
+        def _(zz=zz):
+            pl.semaphore_signal(barrier, inc=1, device_id=at_plane(zz), device_id_type=MESH)
+
+    def tell(which, peer):
+        pl.semaphore_signal(entered.at[which], inc=1, device_id=peer, device_id_type=MESH)
 
     loads = [
         pltpu.make_async_copy(gate_hbm.at[0], w_in.at[:, pl.ds(0, inner)], load_sem.at[0]),
@@ -149,6 +157,12 @@
     ]
     for load in loads:
         load.start()
+
+    @pl.when(z == last)
+    def _():
+        pl.semaphore_wait(barrier, n_tp + last)
+        tell(1, at_plane(0))
+        tell(0, at_plane(1))
 
     inputs[0].wait()
     first = ids_ref[0:1, :]
@@ -173,51 +187,37 @@
     outgoing[...] = sorted_rows.reshape(n_plane, cap, width)
     rows[q, x, z] = outgoing[z]
 
-    inputs[2].wait()
-    inputs[3].wait()
-    weights = expert_ref[...]
-    share = group_ref[...] * weights / jnp.sum(weights, axis=0, keepdims=True)
-    even = (first & 1) == 0
-    for k in range(2):
-        chosen = jnp.where(even, share[k:k + 1, :], share[1 - k:2 - k, :])
-        by_token = jnp.transpose(jnp.broadcast_to(chosen, (tok, tok)))
-        share_out[k:k + 1, :] = jnp.sum(jnp.where(to_token, by_token, zero), axis=0, keepdims=True)
-    share_in[z] = share_out[...]
-
-    pl.semaphore_wait(barrier, 5 + inside)
-
-    def tell(which, peer):
-        pl.semaphore_signal(entered.at[which], inc=1, device_id=peer, device_id_type=MESH)
-
-    @pl.when(inside == 1)
+    @pl.when(z < last)
     def _():
-        tell(0, at_plane(z1))
-        tell(0, at_plane(outer))
-
-    started = []
-
-    def copy(src, dst, sems, recvs, peer):
-        return pltpu.make_async_remote_copy(
-            src_ref=src, dst_ref=dst, send_sem=sems, recv_sem=recvs,
+        pl.semaphore_wait(barrier, n_tp + 1 + z)
+
+    @pl.when(z == 1)
+    def _():
+        tell(0, at_plane(0))
+
+    def start(src, dst, group, arrival, peer):
+        pltpu.make_async_remote_copy(
+            src_ref=src, dst_ref=dst, send_sem=send_sem.at[group], recv_sem=arrival,
             device_id=peer, device_id_type=MESH,
-        )
-
-    def send_between(src, dst, kind, there, here, peer):
-        c = copy(src, dst, send_sem.at[kind, there], recv_sem.at[kind, here], peer)
-        c.start()
-        started.append(c)
-
-    def send(block, kind, zz, peer):
-        send_between(block, block, kind, zz, zz, peer)
-
-    def arrived(dst, kind, zz):
-        copy(dst, dst, send_sem.at[kind, zz], recv_sem.at[kind, zz], core_peer).wait_recv()
+        ).start()
+
+    def send(block, kind, zz, peer, group=IN_PLANE):
+        start(block, block, group, recv_sem.at[kind, zz], peer)
+
+    def landed(ref, arrival):
+        pltpu.make_async_copy(ref, ref, arrival).wait()
+
+    def arrived(ref, kind, zz):
+        landed(ref, recv_sem.at[kind, zz])
 
     low, high = pl.ds(0, half), pl.ds(half, half)
 
     def to_plane(zz):
         for part, kind in ((low, TO_PLANE), (high, TO_PLANE_2)):
-            send_between(outgoing.at[zz, part], rows.at[q, x, z, part], kind, zz, z, at_plane(zz))
+            start(
+                outgoing.at[zz, part], rows.at[q, x, z, part], OFF_PLANE, recv_sem.at[kind, z],
+                at_plane(zz),
+            )
 
     def spread_low(zz):
         block = rows.at[q, x, zz]
@@ -230,7 +230,7 @@
         arrived(block.at[high], TO_PLANE_2, zz)
         send(block.at[high], ACROSS_Y, zz, y_peer)
         send(block.at[high], ACROSS_X2, zz, x_peer)
-        send(block, CORE_OWN, zz, core_peer)
+        send(block, CORE, zz, core_peer, TO_CORE)
 
     def spread_own():
         block = rows.at[q, x, z]
@@ -238,7 +238,7 @@
         send(block.at[high], ACROSS_Y, z, y_peer)
         send(block.at[high], ACROSS_X2, z, x_peer)
         send(block.at[low], ACROSS_Y2, z, y_peer)
-        send(block, CORE_OWN, z, core_peer)
+        send(block, CORE, z, core_peer, TO_CORE)
 
     def pass_on(zz):
         over_x, over_y = rows.at[q, ox, zz], rows.at[q_y, x, zz]
@@ -247,39 +247,36 @@
         arrived(over_y.at[high], ACROSS_Y, zz)
         send(over_y.at[high], RELAY_X, zz, x_peer)
         arrived(over_x.at[high], ACROSS_X2, zz)
-        send(over_x, CORE_X, zz, core_peer)
+        send(over_x, CORE, zz, core_peer, TO_CORE)
         arrived(over_y.at[low], ACROSS_Y2, zz)
-        send(over_y, CORE_Y, zz, core_peer)
+        send(over_y, CORE, zz, core_peer, TO_CORE)
 
     def pass_relayed(zz):
         block = rows.at[q_y, ox, zz]
         arrived(block.at[low], RELAY_Y, zz)
-        send(block.at[low], CORE_RY, zz, core_peer)
+        send(block.at[low], CORE, zz, core_peer, TO_CORE)
         arrived(block.at[high], RELAY_X, zz)
-        send(block.at[high], CORE_RX, zz, core_peer)
-
-    def sums_of(zz, quarter):
-        part = jnp.concatenate([rows[quarter, x, zz], rows[quarter, ox, zz]], axis=0)
+        send(block.at[high], CORE, zz, core_peer, TO_CORE)
+
+    def sums_of(blocks, quarter):
+        part = jnp.concatenate(
+            [rows[quarter, column, zz] for zz in blocks for column in (x, ox)], axis=0
+        )
         w = w_in[pl.ds(pl.multiple_of(quarter * width, width), width), :]
         return jnp.dot(part, w, preferred_element_type=F32)
 
-    def make_hidden(zz):
-        total = sums_of(zz, q) + sums_of(zz, q_y)
-        arrived(rows.at[q_core, x, zz], CORE_OWN, zz)
-        arrived(rows.at[q_core, ox, zz], CORE_X, zz)
-        total = total + sums_of(zz, q_core)
-        arrived(rows.at[q_diag, x, zz], CORE_Y, zz)
-        block = rows.at[q_diag, ox, zz]
-        arrived(block.at[low], CORE_RY, zz)
-        arrived(block.at[high], CORE_RX, zz)
-        total = total + sums_of(zz, q_diag)
+    def make_hidden(*blocks):
+        total = sums_of(blocks, q) + sums_of(blocks, q_y)
+        for zz in blocks:
+            arrived(rows.at[pl.ds(0, 2), :, zz], CORE, zz)
+        total = total + sums_of(blocks, q_core) + sums_of(blocks, q_diag)
         gate, up = total[:, :inner], total[:, inner:]
-        hidden[zz, q] = (gate / (1.0 + jnp.exp(-gate)) * up).astype(BF16)
-        block = hidden.at[zz, q]
-        for d, peer in ((2, y_peer), (3, diag_peer), (1, core_peer)):
-            c = copy(block, block, hidden_send.at[d, zz], hidden_recv.at[d, zz], peer)
-            c.start()
-            started.append(c)
+        made = (gate / (1.0 + jnp.exp(-gate)) * up).astype(BF16)
+        for i, zz in enumerate(blocks):
+            hidden[zz, q] = made[2 * cap * i:2 * cap * (i + 1)]
+            block = hidden.at[zz, q]
+            for peer in (y_peer, diag_peer, core_peer):
+                send(block, HIDDEN, zz, peer, HIDDENS)
 
     lane = lax.broadcasted_iota(jnp.int32, (cap, 128), 1)
     place = lax.broadcasted_iota(jnp.int32, (cap, 128), 0) + z * cap
@@ -291,22 +288,34 @@
 
     is_first = x == 0
 
-    def project(zz):
-        even_share, odd_share = column_of(share_in[zz, 0:1]), column_of(share_in[zz, 1:2])
-        share_own = jnp.where(is_first, even_share, odd_share)
-        share_far[zz] = jnp.broadcast_to(jnp.where(is_first, odd_share, even_share), (cap, 128))
-        for d in range(1, n_tp):
-            block = hidden.at[zz, flip(q, d)]
-            copy(block, block, hidden_send.at[d, zz], hidden_recv.at[d, zz], core_peer).wait_recv()
-        h = jnp.concatenate([hidden[zz, t] for t in range(n_tp)], axis=1)
+    def project(*blocks):
+        for zz in blocks:
+            arrived(hidden.at[zz, pl.ds(0, n_tp - 1)], HIDDEN, zz)
+        h = jnp.concatenate(
+            [
+                jnp.concatenate([hidden[zz, t] for t in range(n_tp)], axis=1)
+                for zz in blocks
+            ],
+            axis=0,
+        )
         result = jnp.dot(h, w_out[...], preferred_element_type=F32).astype(BF16)
-        result_out[zz] = result[cap:]
-        for part, kind in ((low, RESULT), (high, RESULT_2)):
-            send_between(result_out.at[zz, part], result_in.at[zz, part], kind, zz, zz, x_peer)
-        own_part[zz] = result[:cap].astype(F32) * share_own
+        for i, zz in enumerate(blocks):
+            at = 2 * cap * i
+            result_out[zz] = result[at + cap:at + 2 * cap]
+            for part, kind in ((low, RESULT), (high, RESULT_2)):
+                start(
+                    result_out.at[zz, part], result_in.at[zz, part], RESULTS,
+                    recv_sem.at[kind, zz], x_peer,
+                )
+        for i, zz in enumerate(blocks):
+            at = 2 * cap * i
+            even_share, odd_share = column_of(share_in[zz, 0:1]), column_of(share_in[zz, 1:2])
+            share_own = jnp.where(is_first, even_share, odd_share)
+            share_far[zz] = jnp.broadcast_to(jnp.where(is_first, odd_share, even_share), (cap, 128))
+            own_part[zz] = result[at:at + cap].astype(F32) * share_own
 
     def give_back(zz, own=False):
-        for part, at, kind, home in ((low, 0, RESULT, BACK), (high, half, RESULT_2, BACK_2)):
+        for part, at, kind in ((low, 0, RESULT), (high, half, RESULT_2)):
             arrived(result_in.at[zz, part], kind, zz)
             scaled = result_in[zz, at:at + half].astype(F32) * share_far[zz, at:at + half][:, 0:1]
             routed = (own_part[zz, at:at + half] + scaled).astype(BF16)
@@ -314,8 +323,9 @@
                 back_in[z, at:at + half] = routed
             else:
                 back_out[zz, at:at + half] = routed
-                send_between(
-                    back_out.at[zz, part], back_in.at[z, part], home, zz, z, at_plane(zz)
+                start(
+                    back_out.at[zz, part], back_in.at[z, part], OFF_PLANE, once_sem.at[BACK],
+                    at_plane(zz),
                 )
         routed = back_in[z] if own else back_out[zz]
         mixed = residual_scale * rows[q, x, zz].astype(F32) + routed.astype(F32)
@@ -328,79 +338,86 @@
             )
         for d in (2, 3, 1, 0):
             if own and not d:
-                stats_in[z, q] = stats_out[z]
+                stats_in[z * n_tp + q] = stats_out[z]
                 continue
-            c = copy(
-                stats_out.at[zz], stats_in.at[z, q], stats_send.at[d, zz], stats_recv.at[d, z],
+            start(
+                stats_out.at[zz], stats_in.at[z * n_tp + q], STAT, once_sem.at[STATS],
                 (zz * 2 + x, flip(q, d)),
             )
-            c.start()
-            started.append(c)
-
-    to_plane(z1)
+
+    def make_shares():
+        inputs[2].wait()
+        inputs[3].wait()
+        weights = expert_ref[...]
+        share = group_ref[...] * weights / jnp.sum(weights, axis=0, keepdims=True)
+        even = (first & 1) == 0
+        for k in range(2):
+            chosen = jnp.where(even, share[k:k + 1, :], share[1 - k:2 - k, :])
+            by_token = jnp.transpose(jnp.broadcast_to(chosen, (tok, tok)))
+            share_out[k:k + 1, :] = jnp.sum(jnp.where(to_token, by_token, zero), axis=0, keepdims=True)
+        share_in[z] = share_out[...]
+        for zz in (z1, z2, z3):
+            start(share_out, share_in.at[z], SHARE, once_sem.at[SHARES], at_plane(zz))
+
+    to_plane(t1)
     spread_own()
-    pl.semaphore_wait(entered.at[0], 1)
-
-    @pl.when(inside == 1)
+
+    @pl.when(z == 0)
     def _():
-        tell(1, at_plane(outer))
-
-    to_plane(z2)
-
-    @pl.when(inside == 0)
+        pl.semaphore_wait(entered.at[0], 1)
+
+    to_plane(t2)
+
+    @pl.when(z == 0)
     def _():
         pl.semaphore_wait(entered.at[1], 1)
 
-    to_plane(z3)
-    for zz in (z1, z2, z3):
-        send_between(share_out, share_in.at[z], SHARES, zz, z, at_plane(zz))
-
+    @pl.when(z == 1)
+    def _():
+        pl.semaphore_wait(entered.at[0], 1)
+
+    to_plane(t3)
     spread_low(z1)
     pass_on(z)
     spread_high(z1)
+    make_shares()
     spread_low(z2)
     spread_high(z2)
+    pass_relayed(z)
+    pass_on(z1)
+    spread_low(z3)
+    spread_high(z3)
     loads[0].wait()
     loads[1].wait()
-    pass_relayed(z)
-    pass_on(z1)
     make_hidden(z)
     pass_relayed(z1)
     pass_on(z2)
-    spread_low(z3)
-    spread_high(z3)
     make_hidden(z1)
+    pass_on(z3)
     loads[2].wait()
-    for zz in (z1, z2, z3):
-        arrived(share_in.at[zz], SHARES, zz)
+    landed(share_in.at[pl.ds(0, n_plane - 1)], once_sem.at[SHARES])
+    project(z)
     pass_relayed(z2)
-    project(z)
-    pass_on(z3)
     make_hidden(z2)
     project(z1)
     pass_relayed(z3)
-    give_back(z, own=True)
     make_hidden(z3)
     project(z2)
+    give_back(z, own=True)
     give_back(z1)
     project(z3)
     give_back(z2)
     give_back(z3)
 
-    for zz in (z1, z2, z3):
-        arrived(back_in.at[zz, low], BACK, zz)
-        arrived(back_in.at[zz, high], BACK_2, zz)
+    landed(back_in.at[pl.ds(0, n_plane - 1)], once_sem.at[BACK])
     routed = jnp.dot(
         jnp.where(to_token, one, zero).astype(BF16),
         back_in[...].reshape(tok, width),
         preferred_element_type=F32,
     )
     mixed = residual_scale * tokens_ref[...].astype(F32) + routed
-    for d in range(n_tp):
-        for zz in (z, z1, z2, z3) if d else (z1, z2, z3):
-            block = stats_in.at[zz, flip(q, d)]
-            copy(block, block, stats_send.at[d, zz], stats_recv.at[d, zz], core_peer).wait_recv()
-    pieces = [sum(stats_in[zz, t] for zz in range(n_plane)) for t in range(n_tp)]
+    landed(stats_in.at[pl.ds(0, n_plane * n_tp - 1)], once_sem.at[STATS])
+    pieces = [sum(stats_in[zz * n_tp + t] for zz in range(n_plane)) for t in range(n_tp)]
     full = width * n_tp
     center = sum(p[0:1] for p in pieces) / full
     spread = sum(p[1:2] + width * jnp.square(p[0:1] / width - center) for p in pieces) / full
@@ -414,8 +431,16 @@
     normed_out[...] = (
         (mixed - center) * scale * gain_ref[...] + bias_ref[...]
     ).astype(BF16)
-    for c in started:
-        c.wait_send()
+    for group, ref in (
+        (TO_CORE, rows.at[pl.ds(0, 2)]),
+        (IN_PLANE, rows.at[pl.ds(0, 3), 0]),
+        (OFF_PLANE, rows.at[pl.ds(0, 2), 0, pl.ds(0, n_plane - 1)]),
+        (RESULTS, result_out),
+        (HIDDENS, hidden.at[:, pl.ds(0, n_tp - 1)]),
+        (SHARE, share_in.at[pl.ds(0, n_plane - 1)]),
+        (STAT, stats_in.at[pl.ds(0, n_plane * n_tp - 1)]),
+    ):
+        landed(ref, send_sem.at[group])
 
 
 def pair_groups(
@@ -454,13 +479,10 @@
             pltpu.VMEM((n_plane, cap, width), BF16),
             pltpu.VMEM((n_plane, cap, width), BF16),
             pltpu.VMEM((n_plane, 2, tok), F32),
-            pltpu.VMEM((n_plane, n_tp, 2, tok), F32),
+            pltpu.VMEM((n_plane * n_tp, 2, tok), F32),
+            pltpu.SemaphoreType.DMA((7,)),
             pltpu.SemaphoreType.DMA((KINDS, n_plane)),
-            pltpu.SemaphoreType.DMA((KINDS, n_plane)),
-            pltpu.SemaphoreType.DMA((n_tp, n_plane)),
-            pltpu.SemaphoreType.DMA((n_tp, n_plane)),
-            pltpu.SemaphoreType.DMA((n_tp, n_plane)),
-            pltpu.SemaphoreType.DMA((n_tp, n_plane)),
+            pltpu.SemaphoreType.DMA((3,)),
             pltpu.SemaphoreType.DMA((9,)),
             pltpu.SemaphoreType.REGULAR((2,)),
         ],

time: 39 us -> 35.4 us (0.908)
  Pallas kernels: 38.1 us -> 34.5 us
    pallas_call x1, Pallas kernels: 38.1 us -> 34.5 us  [pair_groups(): pl.pallas_call(functools.partial(layer_kernel, n_plane, n_tp), out_shape=...]
where the time goes in v2:
time: 35.4 us; the launch traced here: 35.2 us
  Pallas kernels  34.5 us (97%)
  local copies, waits for them, and re-layouts  0.71 us (2%)
    pallas_call x1, Pallas kernels, pair_groups(): pl.pallas_call(functools.partial(layer_kernel, n_plane, n_tp), out_shape=...  34.5 us

profile of v2, /device:TPU:0, one launch (start us, length us, event | category | flops | bytes accessed | tf_op | source)
XLA Modules:
  0.0 35.2 jit_solution(943476912302809464)
XLA Ops:
  0.0 34.5 %layer.1 = bf16[128,1024]{1,0:T(8,128)(2,1)S(1)} custom-call(bf16[128,1024]{1,0:T(8,128)(2,1)} %tokens_hbm.1, s32[2,128]{1,0:T(2,128)} %bitcast.7, f32[1,128]{1,0:T(1,128)} %bitcast.9, f32[2,128]{1,0:T(2,128)} %bitcast.8, bf16[1,4096,128]{2,1,0:T(8,128)(2,1)} %gate_hbm.1, bf16[1,4096,128]{2,1,0:T(8,128)(2,1)} %up_hbm.1, bf16[1,512,1024]{2,1,0:T(8,128)(2,1)} %down_hbm.1, ...), custom_call_target="tpu_custom_call" | custom-call | tf_op jit(solution)/shard_map/layer/pallas_call | solution.py:456
  34.5 0.7 %copy.11 = bf16[128,1024]{1,0:T(8,128)(2,1)} copy(bf16[128,1024]{1,0:T(8,128)(2,1)S(1)} %layer.1) | data formatting | bytes 524288

commit v3 on v2

--- a/solution.py
+++ b/solution.py
@@ -78,7 +78,7 @@
 MESH = pl.DeviceIdType.MESH
 F32 = jnp.float32
 BF16 = jnp.bfloat16
-(TO_PLANE, TO_PLANE_2, ACROSS_X, ACROSS_Y, ACROSS_X2, ACROSS_Y2, RELAY_X, RELAY_Y, CORE, HIDDEN,
+(FROM_LOWER, FROM_UPPER, ACROSS_X, ACROSS_Y, ACROSS_X2, ACROSS_Y2, RELAY_X, RELAY_Y, CORE, HIDDEN,
  RESULT, RESULT_2) = range(12)
 KINDS = 12
 BACK, SHARES, STATS = range(3)
@@ -111,6 +111,12 @@
     core_peer, y_peer, diag_peer = (ep, q_core), (ep, q_y), (ep, q_diag)
     x_peer = (z * 2 + ox, q)
 
+    upper = lax.rem(q, 2)
+    q_up = q - upper + 1
+    q_low = q_up - 1
+    q_up_y = flip(q_up, 2)
+    q_low_y = q_up_y - 1
+
     def at_plane(zz):
         return (zz * 2 + x, q)
 
@@ -120,8 +126,12 @@
     t2 = n_plane // 2 - lax.div(z, 2)
     t3 = last - lax.div(z, last)
     z1 = z - 1 + 2 * bottom
-    z3 = last - last * lax.div(z, last)
+    z3 = last - 2 * lax.div(z, last)
     z2 = n_plane * last // 2 - z - z1 - z3
+
+    w1 = z1 * (1 - lax.div(z, 2))
+    w3 = z3
+    w2 = n_plane * last // 2 - z - w1 - w3
 
     tok, width = tokens_ref.shape
     cap = tok // n_plane
@@ -145,7 +155,8 @@
 
         @pl.when((zz > z) | (zz == z - 1))
         def _(zz=zz):
-            pl.semaphore_signal(barrier, inc=1, device_id=at_plane(zz), device_id_type=MESH)
+            for peer in (at_plane(zz), (zz * 2 + x, q_core)):
+                pl.semaphore_signal(barrier, inc=1, device_id=peer, device_id_type=MESH)
 
     def tell(which, peer):
         pl.semaphore_signal(entered.at[which], inc=1, device_id=peer, device_id_type=MESH)
@@ -160,7 +171,7 @@
 
     @pl.when(z == last)
     def _():
-        pl.semaphore_wait(barrier, n_tp + last)
+        pl.semaphore_wait(barrier, n_tp + 2 * last)
         tell(1, at_plane(0))
         tell(0, at_plane(1))
 
@@ -185,11 +196,15 @@
         jnp.where(to_slot, one, zero).astype(BF16), tokens_ref[...], preferred_element_type=F32
     ).astype(BF16)
     outgoing[...] = sorted_rows.reshape(n_plane, cap, width)
-    rows[q, x, z] = outgoing[z]
+
+    @pl.when(upper == 1)
+    def _():
+        rows[q, x, z] = outgoing[z]
+
 
     @pl.when(z < last)
     def _():
-        pl.semaphore_wait(barrier, n_tp + 1 + z)
+        pl.semaphore_wait(barrier, n_tp + 2 + 2 * z)
 
     @pl.when(z == 1)
     def _():
@@ -213,63 +228,67 @@
     low, high = pl.ds(0, half), pl.ds(half, half)
 
     def to_plane(zz):
-        for part, kind in ((low, TO_PLANE), (high, TO_PLANE_2)):
-            start(
-                outgoing.at[zz, part], rows.at[q, x, z, part], OFF_PLANE, recv_sem.at[kind, z],
-                at_plane(zz),
-            )
+        start(
+            outgoing.at[zz], rows.at[q, x, z], OFF_PLANE, recv_sem.at[FROM_LOWER + upper, z],
+            (zz * 2 + x, q_up),
+        )
+
+    def hand_over():
+        start(outgoing.at[z], rows.at[q, x, z], TO_CORE, recv_sem.at[FROM_LOWER, z], core_peer)
+
+    def to_core(block, zz):
+        send(block, CORE, zz, core_peer, TO_CORE)
+
+    def spread_up(zz):
+        block = rows.at[q_up, x, zz]
+        if zz is not z:
+            arrived(block, FROM_UPPER, zz)
+        send(block, ACROSS_X, zz, x_peer)
+        send(block, ACROSS_Y2, zz, y_peer)
+        to_core(block, zz)
 
     def spread_low(zz):
-        block = rows.at[q, x, zz]
-        arrived(block.at[low], TO_PLANE, zz)
-        send(block.at[low], ACROSS_X, zz, x_peer)
-        send(block.at[low], ACROSS_Y2, zz, y_peer)
-
-    def spread_high(zz):
-        block = rows.at[q, x, zz]
-        arrived(block.at[high], TO_PLANE_2, zz)
-        send(block.at[high], ACROSS_Y, zz, y_peer)
-        send(block.at[high], ACROSS_X2, zz, x_peer)
-        send(block, CORE, zz, core_peer, TO_CORE)
-
-    def spread_own():
-        block = rows.at[q, x, z]
-        send(block.at[low], ACROSS_X, z, x_peer)
-        send(block.at[high], ACROSS_Y, z, y_peer)
-        send(block.at[high], ACROSS_X2, z, x_peer)
-        send(block.at[low], ACROSS_Y2, z, y_peer)
-        send(block, CORE, z, core_peer, TO_CORE)
+        block = rows.at[q_low, x, zz]
+        arrived(block, FROM_LOWER, zz)
+        send(block, ACROSS_Y, zz, y_peer)
+        send(block, ACROSS_X2, zz, x_peer)
+        to_core(block, zz)
 
     def pass_on(zz):
-        over_x, over_y = rows.at[q, ox, zz], rows.at[q_y, x, zz]
-        arrived(over_x.at[low], ACROSS_X, zz)
-        send(over_x.at[low], RELAY_Y, zz, y_peer)
-        arrived(over_y.at[high], ACROSS_Y, zz)
-        send(over_y.at[high], RELAY_X, zz, x_peer)
-        arrived(over_x.at[high], ACROSS_X2, zz)
-        send(over_x, CORE, zz, core_peer, TO_CORE)
-        arrived(over_y.at[low], ACROSS_Y2, zz)
-        send(over_y, CORE, zz, core_peer, TO_CORE)
+        block = rows.at[q_up, ox, zz]
+        arrived(block, ACROSS_X, zz)
+        send(block, RELAY_Y, zz, y_peer)
+        to_core(block, zz)
+        block = rows.at[q_low_y, x, zz]
+        arrived(block, ACROSS_Y, zz)
+        send(block, RELAY_X, zz, x_peer)
+        to_core(block, zz)
+        block = rows.at[q_low, ox, zz]
+        arrived(block, ACROSS_X2, zz)
+        to_core(block, zz)
+        block = rows.at[q_up_y, x, zz]
+        arrived(block, ACROSS_Y2, zz)
+        to_core(block, zz)
 
     def pass_relayed(zz):
-        block = rows.at[q_y, ox, zz]
-        arrived(block.at[low], RELAY_Y, zz)
-        send(block.at[low], CORE, zz, core_peer, TO_CORE)
-        arrived(block.at[high], RELAY_X, zz)
-        send(block.at[high], CORE, zz, core_peer, TO_CORE)
+        for block, kind in (
+            (rows.at[q_up_y, ox, zz], RELAY_Y), (rows.at[q_low_y, ox, zz], RELAY_X),
+        ):
+            arrived(block, kind, zz)
+            to_core(block, zz)
 
     def sums_of(blocks, quarter):
         part = jnp.concatenate(
             [rows[quarter, column, zz] for zz in blocks for column in (x, ox)], axis=0
         )
-        w = w_in[pl.ds(pl.multiple_of(quarter * width, width), width), :]
+        w = w_in[quarter * width:(quarter + 1) * width, :]
         return jnp.dot(part, w, preferred_element_type=F32)
 
-    def make_hidden(*blocks):
-        total = sums_of(blocks, q) + sums_of(blocks, q_y)
-        for zz in blocks:
-            arrived(rows.at[pl.ds(0, 2), :, zz], CORE, zz)
-        total = total + sums_of(blocks, q_core) + sums_of(blocks, q_diag)
+    def make_hidden(*blocks, lower=False):
+        if lower:
+            for zz in blocks:
+                arrived(rows.at[:, :, zz], CORE, zz)
+        total = sum(sums_of(blocks, t) for t in range(n_tp))
         gate, up = total[:, :inner], total[:, inner:]
         made = (gate / (1.0 + jnp.exp(-gate)) * up).astype(BF16)
         for i, zz in enumerate(blocks):
@@ -360,7 +379,14 @@
             start(share_out, share_in.at[z], SHARE, once_sem.at[SHARES], at_plane(zz))
 
     to_plane(t1)
-    spread_own()
+
+    @pl.when(upper == 1)
+    def _():
+        spread_up(z)
+
+    @pl.when(upper == 0)
+    def _():
+        hand_over()
 
     @pl.when(z == 0)
     def _():
@@ -368,46 +394,83 @@
 
     to_plane(t2)
 
+    @pl.when(z >= 2)
+    def _():
+        to_plane(t3)
+
+    @pl.when(upper == 1)
+    def _():
+        spread_low(z)
+
     @pl.when(z == 0)
     def _():
         pl.semaphore_wait(entered.at[1], 1)
-
-    @pl.when(z == 1)
-    def _():
-        pl.semaphore_wait(entered.at[0], 1)
-
-    to_plane(t3)
-    spread_low(z1)
-    pass_on(z)
-    spread_high(z1)
-    make_shares()
-    spread_low(z2)
-    spread_high(z2)
-    pass_relayed(z)
-    pass_on(z1)
-    spread_low(z3)
-    spread_high(z3)
-    loads[0].wait()
-    loads[1].wait()
-    make_hidden(z)
-    pass_relayed(z1)
-    pass_on(z2)
-    make_hidden(z1)
-    pass_on(z3)
-    loads[2].wait()
-    landed(share_in.at[pl.ds(0, n_plane - 1)], once_sem.at[SHARES])
-    project(z)
-    pass_relayed(z2)
-    make_hidden(z2)
-    project(z1)
-    pass_relayed(z3)
-    make_hidden(z3)
-    project(z2)
-    give_back(z, own=True)
-    give_back(z1)
-    project(z3)
-    give_back(z2)
-    give_back(z3)
+        to_plane(t3)
+
+
+    @pl.when(upper == 1)
+    def _():
+        spread_up(z1)
+        pass_on(z)
+        spread_low(z1)
+        @pl.when(z == 1)
+        def _():
+            pl.semaphore_wait(entered.at[0], 1)
+            to_plane(t3)
+
+        make_shares()
+        spread_up(z2)
+        spread_low(z2)
+        pass_relayed(z)
+        pass_on(z1)
+        spread_up(z3)
+        spread_low(z3)
+        loads[0].wait()
+        loads[1].wait()
+        make_hidden(z)
+        pass_relayed(z1)
+        pass_on(z2)
+        make_hidden(z1)
+        pass_on(z3)
+        loads[2].wait()
+        landed(share_in.at[pl.ds(0, n_plane - 1)], once_sem.at[SHARES])
+        project(z)
+        pass_relayed(z2)
+        make_hidden(z2)
+        pass_relayed(z3)
+        make_hidden(z3)
+        project(w1)
+        project(w2)
+        give_back(z, own=True)
+        give_back(w1)
+        project(w3)
+        give_back(w2)
+        give_back(w3)
+
+    @pl.when(upper == 0)
+    def _():
+        @pl.when(z == 1)
+        def _():
+            pl.semaphore_wait(entered.at[0], 1)
+            to_plane(t3)
+
+        make_shares()
+        loads[0].wait()
+        loads[1].wait()
+        make_hidden(z, lower=True)
+        make_hidden(z1, lower=True)
+        loads[2].wait()
+        landed(share_in.at[pl.ds(0, n_plane - 1)], once_sem.at[SHARES])
+        project(z)
+        make_hidden(z2, lower=True)
+        make_hidden(z3, lower=True)
+        project(w1)
+        project(w2)
+        give_back(z, own=True)
+        give_back(w1)
+        project(w3)
+        give_back(w2)
+        give_back(w3)
 
     landed(back_in.at[pl.ds(0, n_plane - 1)], once_sem.at[BACK])
     routed = jnp.dot(
@@ -431,9 +494,16 @@
     normed_out[...] = (
         (mixed - center) * scale * gain_ref[...] + bias_ref[...]
     ).astype(BF16)
+    @pl.when(upper == 1)
+    def _():
+        landed(rows, send_sem.at[TO_CORE])
+        landed(rows.at[pl.ds(0, n_tp - 1)], send_sem.at[IN_PLANE])
+
+    @pl.when(upper == 0)
+    def _():
+        landed(outgoing.at[0], send_sem.at[TO_CORE])
+
     for group, ref in (
-        (TO_CORE, rows.at[pl.ds(0, 2)]),
-        (IN_PLANE, rows.at[pl.ds(0, 3), 0]),
         (OFF_PLANE, rows.at[pl.ds(0, 2), 0, pl.ds(0, n_plane - 1)]),
         (RESULTS, result_out),
         (HIDDENS, hidden.at[:, pl.ds(0, n_tp - 1)]),

time: 35.4 us -> 34.1 us (0.963)
  Pallas kernels: 34.5 us -> 33 us
    pallas_call x1, Pallas kernels: 34.5 us -> 33 us  [pair_groups(): pl.pallas_call(functools.partial(layer_kernel, n_plane, n_tp), out_shape=...]
where the time goes in v3:
time: 34.1 us; the launch traced here: 33.7 us
  Pallas kernels  33 us (97%)
  local copies, waits for them, and re-layouts  0.71 us (2%)
    pallas_call x1, Pallas kernels, pair_groups(): pl.pallas_call(functools.partial(layer_kernel, n_plane, n_tp), out_shape=...  33 us
    unnamed x1, local copies, waits for them, and re-layouts  0.71 us

profile of v3, /device:TPU:0, one launch (start us, length us, event | category | flops | bytes accessed | tf_op | source)
XLA Modules:
  0.0 33.7 jit_solution(5902572981665989298)
XLA Ops:
  0.0 33.0 %layer.1 = bf16[128,1024]{1,0:T(8,128)(2,1)S(1)} custom-call(bf16[128,1024]{1,0:T(8,128)(2,1)} %tokens_hbm.1, s32[2,128]{1,0:T(2,128)} %bitcast.7, f32[1,128]{1,0:T(1,128)} %bitcast.9, f32[2,128]{1,0:T(2,128)} %bitcast.8, bf16[1,4096,128]{2,1,0:T(8,128)(2,1)} %gate_hbm.1, bf16[1,4096,128]{2,1,0:T(8,128)(2,1)} %up_hbm.1, bf16[1,512,1024]{2,1,0:T(8,128)(2,1)} %down_hbm.1, ...), custom_call_target="tpu_custom_call" | custom-call | tf_op jit(solution)/shard_map/layer/pallas_call | solution.py:526
  33.0 0.7 %copy.11 = bf16[128,1024]{1,0:T(8,128)(2,1)} copy(bf16[128,1024]{1,0:T(8,128)(2,1)S(1)} %layer.1) | data formatting | bytes 524288

commit v4 on v3

--- a/solution.py
+++ b/solution.py
@@ -78,9 +78,9 @@
 MESH = pl.DeviceIdType.MESH
 F32 = jnp.float32
 BF16 = jnp.bfloat16
-(FROM_LOWER, FROM_UPPER, ACROSS_X, ACROSS_Y, ACROSS_X2, ACROSS_Y2, RELAY_X, RELAY_Y, CORE, HIDDEN,
- RESULT, RESULT_2) = range(12)
-KINDS = 12
+(FROM_LOWER, FROM_UPPER, ACROSS_X, ACROSS_Y, ACROSS_X2, ACROSS_Y2, RELAY_X, RELAY_Y, CORE, CORE_2,
+ HIDDEN, RESULT, RESULT_2) = range(13)
+KINDS = 13
 BACK, SHARES, STATS = range(3)
 TO_CORE, IN_PLANE, OFF_PLANE, RESULTS, HIDDENS, SHARE, STAT = range(7)
 
@@ -99,7 +99,7 @@
     tokens_hbm, ids_hbm, group_hbm, expert_hbm, gate_hbm, up_hbm, down_hbm, gain_hbm, bias_hbm,
     normed_out,
     tokens_ref, ids_ref, group_ref, expert_ref, gain_ref, bias_ref,
-    w_in, w_out, outgoing, share_out, share_in, share_far, rows, hidden, own_part, result_out,
+    w_in, w_out, outgoing, share_out, share_in, share_far, rows, sums, hidden, own_part, result_out,
     result_in, back_out, back_in, stats_out, stats_in,
     send_sem, recv_sem, once_sem, load_sem, entered,
 ):
@@ -109,7 +109,7 @@
     ox = 1 - x
     q_core, q_y, q_diag = flip(q, 1), flip(q, 2), flip(q, 3)
     core_peer, y_peer, diag_peer = (ep, q_core), (ep, q_y), (ep, q_diag)
-    x_peer = (z * 2 + ox, q)
+    x_peer, corner_peer = (z * 2 + ox, q), (z * 2 + ox, flip(q, 2))
 
     upper = lax.rem(q, 2)
     q_up = q - upper + 1
@@ -126,12 +126,8 @@
     t2 = n_plane // 2 - lax.div(z, 2)
     t3 = last - lax.div(z, last)
     z1 = z - 1 + 2 * bottom
-    z3 = last - 2 * lax.div(z, last)
-    z2 = n_plane * last // 2 - z - z1 - z3
-
-    w1 = z1 * (1 - lax.div(z, 2))
-    w3 = z3
-    w2 = n_plane * last // 2 - z - w1 - w3
+    z2 = last * (1 - lax.div(z, 2))
+    z3 = n_plane * last // 2 - z - z1 - z2
 
     tok, width = tokens_ref.shape
     cap = tok // n_plane
@@ -239,29 +235,35 @@
     def to_core(block, zz):
         send(block, CORE, zz, core_peer, TO_CORE)
 
-    def spread_up(zz):
+    def spread_up(zz, corner=False):
         block = rows.at[q_up, x, zz]
         if zz is not z:
             arrived(block, FROM_UPPER, zz)
+        if corner:
+            send(block, RELAY_Y, zz, corner_peer)
         send(block, ACROSS_X, zz, x_peer)
         send(block, ACROSS_Y2, zz, y_peer)
         to_core(block, zz)
 
-    def spread_low(zz):
+    def spread_low(zz, corner=False):
         block = rows.at[q_low, x, zz]
         arrived(block, FROM_LOWER, zz)
+        if corner:
+            send(block, RELAY_X, zz, corner_peer)
         send(block, ACROSS_Y, zz, y_peer)
         send(block, ACROSS_X2, zz, x_peer)
         to_core(block, zz)
 
-    def pass_on(zz):
+    def pass_on(zz, corner=False):
         block = rows.at[q_up, ox, zz]
         arrived(block, ACROSS_X, zz)
-        send(block, RELAY_Y, zz, y_peer)
+        if not corner:
+            send(block, RELAY_Y, zz, y_peer)
         to_core(block, zz)
         block = rows.at[q_low_y, x, zz]
         arrived(block, ACROSS_Y, zz)
-        send(block, RELAY_X, zz, x_peer)
+        if not corner:
+            send(block, RELAY_X, zz, x_peer)
         to_core(block, zz)
         block = rows.at[q_low, ox, zz]
         arrived(block, ACROSS_X2, zz)
@@ -275,27 +277,27 @@
             (rows.at[q_up_y, ox, zz], RELAY_Y), (rows.at[q_low_y, ox, zz], RELAY_X),
         ):
             arrived(block, kind, zz)
-            to_core(block, zz)
-
-    def sums_of(blocks, quarter):
-        part = jnp.concatenate(
-            [rows[quarter, column, zz] for zz in blocks for column in (x, ox)], axis=0
-        )
-        w = w_in[quarter * width:(quarter + 1) * width, :]
+            send(block, CORE_2, zz, core_peer, TO_CORE)
+
+    def sums_of(zz, quarter):
+        part = jnp.concatenate([rows[quarter, x, zz], rows[quarter, ox, zz]], axis=0)
+        w = w_in[pl.ds(pl.multiple_of(quarter * width, width), width), :]
         return jnp.dot(part, w, preferred_element_type=F32)
 
-    def make_hidden(*blocks, lower=False):
+    def begin_hidden(zz, lower=False):
         if lower:
-            for zz in blocks:
-                arrived(rows.at[:, :, zz], CORE, zz)
-        total = sum(sums_of(blocks, t) for t in range(n_tp))
+            arrived(rows.at[pl.ds(0, n_tp - 1), :, zz], CORE, zz)
+        sums[zz] = sums_of(zz, q_low) + sums_of(zz, q_up)
+
+    def make_hidden(zz, lower=False):
+        if lower:
+            arrived(rows.at[0, :, zz], CORE_2, zz)
+        total = sums[zz] + (sums_of(zz, q_low_y) + sums_of(zz, q_up_y))
         gate, up = total[:, :inner], total[:, inner:]
-        made = (gate / (1.0 + jnp.exp(-gate)) * up).astype(BF16)
-        for i, zz in enumerate(blocks):
-            hidden[zz, q] = made[2 * cap * i:2 * cap * (i + 1)]
-            block = hidden.at[zz, q]
-            for peer in (y_peer, diag_peer, core_peer):
-                send(block, HIDDEN, zz, peer, HIDDENS)
+        hidden[zz, q] = (gate / (1.0 + jnp.exp(-gate)) * up).astype(BF16)
+        block = hidden.at[zz, q]
+        for peer in (y_peer, diag_peer, core_peer):
+            send(block, HIDDEN, zz, peer, HIDDENS)
 
     lane = lax.broadcasted_iota(jnp.int32, (cap, 128), 1)
     place = lax.broadcasted_iota(jnp.int32, (cap, 128), 0) + z * cap
@@ -419,33 +421,82 @@
             to_plane(t3)
 
         make_shares()
-        spread_up(z2)
-        spread_low(z2)
+
+        @pl.when(z < 2)
+        def _():
+            spread_up(z2)
+            spread_low(z2)
+
+        @pl.when(z >= 2)
+        def _():
+            spread_up(z2, corner=True)
+            spread_low(z2, corner=True)
+
         pass_relayed(z)
         pass_on(z1)
         spread_up(z3)
         spread_low(z3)
         loads[0].wait()
         loads[1].wait()
+        begin_hidden(z)
         make_hidden(z)
+
+        @pl.when(z >= 2)
+        def _():
+            pass_on(z2, corner=True)
+            begin_hidden(z2)
+            pass_relayed(z2)
+            make_hidden(z2)
+
+        begin_hidden(z1)
         pass_relayed(z1)
-        pass_on(z2)
         make_hidden(z1)
-        pass_on(z3)
-        loads[2].wait()
-        landed(share_in.at[pl.ds(0, n_plane - 1)], once_sem.at[SHARES])
-        project(z)
-        pass_relayed(z2)
-        make_hidden(z2)
-        pass_relayed(z3)
-        make_hidden(z3)
-        project(w1)
-        project(w2)
-        give_back(z, own=True)
-        give_back(w1)
-        project(w3)
-        give_back(w2)
-        give_back(w3)
+
+
+        @pl.when(z >= 2)
+        def _():
+            pass_on(z3)
+            loads[2].wait()
+            landed(share_in.at[pl.ds(0, n_plane - 1)], once_sem.at[SHARES])
+            project(z)
+            begin_hidden(z3)
+
+        @pl.when(z < 2)
+        def _():
+            pass_on(z2)
+            begin_hidden(z2)
+            pass_on(z3)
+            loads[2].wait()
+            landed(share_in.at[pl.ds(0, n_plane - 1)], once_sem.at[SHARES])
+            project(z)
+            begin_hidden(z3)
+            pass_relayed(z2)
+            make_hidden(z2)
+
+
+        @pl.when(z >= 2)
+        def _():
+            project(z2)
+            pass_relayed(z3)
+            make_hidden(z3)
+            project(z1)
+            give_back(z2)
+            project(z3)
+            give_back(z, own=True)
+            give_back(z1)
+            give_back(z3)
+
+        @pl.when(z < 2)
+        def _():
+            pass_relayed(z3)
+            make_hidden(z3)
+            project(z1)
+            project(z2)
+            give_back(z1)
+            project(z3)
+            give_back(z, own=True)
+            give_back(z2)
+            give_back(z3)
 
     @pl.when(upper == 0)
     def _():
@@ -457,20 +508,46 @@
         make_shares()
         loads[0].wait()
         loads[1].wait()
+        begin_hidden(z, lower=True)
         make_hidden(z, lower=True)
-        make_hidden(z1, lower=True)
-        loads[2].wait()
-        landed(share_in.at[pl.ds(0, n_plane - 1)], once_sem.at[SHARES])
-        project(z)
-        make_hidden(z2, lower=True)
-        make_hidden(z3, lower=True)
-        project(w1)
-        project(w2)
-        give_back(z, own=True)
-        give_back(w1)
-        project(w3)
-        give_back(w2)
-        give_back(w3)
+
+        @pl.when(z >= 2)
+        def _():
+            begin_hidden(z2, lower=True)
+            make_hidden(z2, lower=True)
+            begin_hidden(z1, lower=True)
+            make_hidden(z1, lower=True)
+            loads[2].wait()
+            landed(share_in.at[pl.ds(0, n_plane - 1)], once_sem.at[SHARES])
+            project(z)
+            project(z2)
+            begin_hidden(z3, lower=True)
+            make_hidden(z3, lower=True)
+            project(z1)
+            give_back(z2)
+            project(z3)
+            give_back(z, own=True)
+            give_back(z1)
+            give_back(z3)
+
+        @pl.when(z < 2)
+        def _():
+            begin_hidden(z1, lower=True)
+            make_hidden(z1, lower=True)
+            loads[2].wait()
+            landed(share_in.at[pl.ds(0, n_plane - 1)], once_sem.at[SHARES])
+            project(z)
+            begin_hidden(z2, lower=True)
+            make_hidden(z2, lower=True)
+            begin_hidden(z3, lower=True)
+            make_hidden(z3, lower=True)
+            project(z1)
+            project(z2)
+            give_back(z1)
+            project(z3)
+            give_back(z, own=True)
+            give_back(z2)
+            give_back(z3)
 
     landed(back_in.at[pl.ds(0, n_plane - 1)], once_sem.at[BACK])
     routed = jnp.dot(
@@ -542,6 +619,7 @@
             pltpu.VMEM((n_plane, 2, tok), F32),
             pltpu.VMEM((n_plane, cap, 128), F32),
             pltpu.VMEM((n_tp, 2, n_plane, cap, width), BF16),
+            pltpu.VMEM((n_plane, 2 * cap, 2 * inner), F32),
             pltpu.VMEM((n_plane, n_tp, 2 * cap, inner), BF16),
             pltpu.VMEM((n_plane, cap, width), F32),
             pltpu.VMEM((n_plane, cap, width), BF16),

time: 34.1 us -> 31.9 us (0.935)
  the two profiles are of different devices: /device:TPU:0 before, /device:TPU:9 now
where the time goes in v4:
time: 31.9 us; the launch traced here: 31.8 us
  Pallas kernels  31.1 us (97%)
  local copies, waits for them, and re-layouts  0.71 us (2%)
    pallas_call x1, Pallas kernels, pair_groups(): pl.pallas_call(functools.partial(layer_kernel, n_plane, n_tp), out_shape=...  31.1 us
    unnamed x1, local copies, waits for them, and re-layouts  0.71 us

profile of v4, /device:TPU:9, one launch (start us, length us, event | category | flops | bytes accessed | tf_op | source)
XLA Modules:
  0.0 31.8 jit_solution(6538466173061613142)
XLA Ops:
  0.0 31.1 %layer.1 = bf16[128,1024]{1,0:T(8,128)(2,1)S(1)} custom-call(bf16[128,1024]{1,0:T(8,128)(2,1)} %tokens_hbm.1, s32[2,128]{1,0:T(2,128)} %bitcast.7, f32[1,128]{1,0:T(1,128)} %bitcast.9, f32[2,128]{1,0:T(2,128)} %bitcast.8, bf16[1,4096,128]{2,1,0:T(8,128)(2,1)} %gate_hbm.1, bf16[1,4096,128]{2,1,0:T(8,128)(2,1)} %up_hbm.1, bf16[1,512,1024]{2,1,0:T(8,128)(2,1)} %down_hbm.1, ...), custom_call_target="tpu_custom_call" | custom-call | tf_op jit(solution)/shard_map/layer/pallas_call | solution.py:603
  31.1 0.7 %copy.11 = bf16[128,1024]{1,0:T(8,128)(2,1)} copy(bf16[128,1024]{1,0:T(8,128)(2,1)S(1)} %layer.1) | data formatting | bytes 524288

commit v5 on v4

--- a/solution.py
+++ b/solution.py
@@ -79,8 +79,9 @@
 F32 = jnp.float32
 BF16 = jnp.bfloat16
 (FROM_LOWER, FROM_UPPER, ACROSS_X, ACROSS_Y, ACROSS_X2, ACROSS_Y2, RELAY_X, RELAY_Y, CORE, CORE_2,
- HIDDEN, RESULT, RESULT_2) = range(13)
-KINDS = 13
+ HIDDEN, RESULT) = range(12)
+PARTS = 2
+KINDS = RESULT + PARTS
 BACK, SHARES, STATS = range(3)
 TO_CORE, IN_PLANE, OFF_PLANE, RESULTS, HIDDENS, SHARE, STAT = range(7)
 
@@ -131,7 +132,7 @@
 
     tok, width = tokens_ref.shape
     cap = tok // n_plane
-    half = cap // 2
+    step = cap // PARTS
     inner = gate_hbm.shape[2]
 
     inputs = [
@@ -164,12 +165,6 @@
     ]
     for load in loads:
         load.start()
-
-    @pl.when(z == last)
-    def _():
-        pl.semaphore_wait(barrier, n_tp + 2 * last)
-        tell(1, at_plane(0))
-        tell(0, at_plane(1))
 
     inputs[0].wait()
     first = ids_ref[0:1, :]
@@ -198,6 +193,12 @@
         rows[q, x, z] = outgoing[z]
 
 
+    @pl.when(z == last)
+    def _():
+        pl.semaphore_wait(barrier, n_tp + 2 * last)
+        tell(1, at_plane(0))
+        tell(0, at_plane(1))
+
     @pl.when(z < last)
     def _():
         pl.semaphore_wait(barrier, n_tp + 2 + 2 * z)
@@ -220,8 +221,6 @@
 
     def arrived(ref, kind, zz):
         landed(ref, recv_sem.at[kind, zz])
-
-    low, high = pl.ds(0, half), pl.ds(half, half)
 
     def to_plane(zz):
         start(
@@ -323,7 +322,8 @@
         for i, zz in enumerate(blocks):
             at = 2 * cap * i
             result_out[zz] = result[at + cap:at + 2 * cap]
-            for part, kind in ((low, RESULT), (high, RESULT_2)):
+            for n in range(PARTS):
+                part, kind = pl.ds(n * step, step), RESULT + n
                 start(
                     result_out.at[zz, part], result_in.at[zz, part], RESULTS,
                     recv_sem.at[kind, zz], x_peer,
@@ -336,14 +336,15 @@
             own_part[zz] = result[at:at + cap].astype(F32) * share_own
 
     def give_back(zz, own=False):
-        for part, at, kind in ((low, 0, RESULT), (high, half, RESULT_2)):
+        for i in range(PARTS):
+            at, part, kind = i * step, pl.ds(i * step, step), RESULT + i
             arrived(result_in.at[zz, part], kind, zz)
-            scaled = result_in[zz, at:at + half].astype(F32) * share_far[zz, at:at + half][:, 0:1]
-            routed = (own_part[zz, at:at + half] + scaled).astype(BF16)
+            scaled = result_in[zz, at:at + step].astype(F32) * share_far[zz, at:at + step][:, 0:1]
+            routed = (own_part[zz, at:at + step] + scaled).astype(BF16)
             if own:
-                back_in[z, at:at + half] = routed
+                back_in[z, at:at + step] = routed
             else:
-                back_out[zz, at:at + half] = routed
+                back_out[zz, at:at + step] = routed
                 start(
                     back_out.at[zz, part], back_in.at[z, part], OFF_PLANE, once_sem.at[BACK],
                     at_plane(zz),
@@ -447,22 +448,29 @@
             begin_hidden(z2)
             pass_relayed(z2)
             make_hidden(z2)
-
-        begin_hidden(z1)
-        pass_relayed(z1)
-        make_hidden(z1)
-
-
-        @pl.when(z >= 2)
-        def _():
+            begin_hidden(z1)
+            pass_relayed(z1)
+            make_hidden(z1)
             pass_on(z3)
             loads[2].wait()
             landed(share_in.at[pl.ds(0, n_plane - 1)], once_sem.at[SHARES])
             project(z)
             begin_hidden(z3)
+            pass_relayed(z3)
+            project(z2)
+            make_hidden(z3)
+            project(z1)
+            give_back(z2)
+            project(z3)
+            give_back(z, own=True)
+            give_back(z1)
+            give_back(z3)
 
         @pl.when(z < 2)
         def _():
+            begin_hidden(z1)
+            pass_relayed(z1)
+            make_hidden(z1)
             pass_on(z2)
             begin_hidden(z2)
             pass_on(z3)
@@ -472,22 +480,6 @@
             begin_hidden(z3)
             pass_relayed(z2)
             make_hidden(z2)
-
-
-        @pl.when(z >= 2)
-        def _():
-            project(z2)
-            pass_relayed(z3)
-            make_hidden(z3)
-            project(z1)
-            give_back(z2)
-            project(z3)
-            give_back(z, own=True)
-            give_back(z1)
-            give_back(z3)
-
-        @pl.when(z < 2)
-        def _():
             pass_relayed(z3)
             make_hidden(z3)
             project(z1)

time: 31.9 us -> 31.7 us (level)
  the two profiles are of different devices: /device:TPU:9 before, /device:TPU:17 now
where the time goes in v5:
time: 31.7 us; the launch traced here: 31.5 us
  Pallas kernels  30.8 us (97%)
  local copies, waits for them, and re-layouts  0.71 us (2%)
    pallas_call x1, Pallas kernels, pair_groups(): pl.pallas_call(functools.partial(layer_kernel, n_plane, n_tp), out_shape=...  30.8 us
    unnamed x1, local copies, waits for them, and re-layouts  0.71 us

profile of v5, /device:TPU:17, one launch (start us, length us, event | category | flops | bytes accessed | tf_op | source)
XLA Modules:
  0.0 31.5 jit_solution(3770299514931078265)
XLA Ops:
  0.0 30.8 %layer.1 = bf16[128,1024]{1,0:T(8,128)(2,1)S(1)} custom-call(bf16[128,1024]{1,0:T(8,128)(2,1)} %tokens_hbm.1, s32[2,128]{1,0:T(2,128)} %bitcast.7, f32[1,128]{1,0:T(1,128)} %bitcast.9, f32[2,128]{1,0:T(2,128)} %bitcast.8, bf16[1,4096,128]{2,1,0:T(8,128)(2,1)} %gate_hbm.1, bf16[1,4096,128]{2,1,0:T(8,128)(2,1)} %up_hbm.1, bf16[1,512,1024]{2,1,0:T(8,128)(2,1)} %down_hbm.1, ...), custom_call_target="tpu_custom_call" | custom-call | tf_op jit(solution)/shard_map/layer/pallas_call | solution.py:595
  30.8 0.7 %copy.11 = bf16[128,1024]{1,0:T(8,128)(2,1)} copy(bf16[128,1024]{1,0:T(8,128)(2,1)S(1)} %layer.1) | data formatting | bytes 524288
